TPU v7x, 256 devices: a whole 4x4x8 slice. The times are simulated.
256 devices in a mesh: sp: 64 (over z, x, core), tp: 4 (over y).
Axes of the slice: x: 4, y: 4, z: 8, core: 2. Of those that a mesh axis runs over, the one named last changes fastest.
Arguments:
- mid: bfloat16 [12288, 2048], P('sp'), may hold values from -6 to 6
- out_grad: bfloat16 [12288, 2048], P('sp'), may hold values from -16 to 16
- expert_ids: int32 [12288, 2], P('sp'), may hold values from 0 to 63, all different within a row; in each aligned block of 192 rows (0 to 191, 192 to 383, ...) at most 9 rows name the same one
- route_weights: float32 [12288, 2], P('sp'), may hold values from 0.1 to 0.9
- gate_proj: bfloat16 [64, 2048, 1024], P('sp', None, 'tp'), may hold values from -0.375 to 0.375
- up_proj: bfloat16 [64, 2048, 1024], P('sp', None, 'tp'), may hold values from -0.375 to 0.375
- down_proj: bfloat16 [64, 1024, 2048], P('sp', 'tp'), may hold values from -0.1875 to 0.1875
- out_proj: bfloat16 [512, 2048], P('tp'), may hold values from -0.25 to 0.25
- branch_gate: bfloat16 [12288, 512], P('sp', 'tp'), may hold values from -6 to 6
- conv_out: bfloat16 [2, 12288, 512], P(None, 'sp', 'tp'), may hold values from -6 to 6
- prior_state: float32 [2, 12288, 512], P(None, 'sp', 'tp'), may hold values from -6 to 6
- rate_gate_w: bfloat16 [2, 8, 64, 64], P(None, 'tp'), may hold values from -0.75 to 0.75
- input_gate_w: bfloat16 [2, 8, 64, 64], P(None, 'tp'), may hold values from -0.75 to 0.75
- decay_param: float32 [2, 512], P(None, 'tp'), may hold values from 4 to 16
- decay_jump: float32 [2, 12288, 512], P(None, 'sp', 'tp'), may hold values from -2 to 0
- conv_taps: bfloat16 [2, 4, 512], P(None, None, 'tp'), may hold values from -3 to 3
Outputs:
- gate_grad: bfloat16 [64, 2048, 1024], P('sp', None, 'tp')
- up_grad: bfloat16 [64, 2048, 1024], P('sp', None, 'tp')
- down_grad: bfloat16 [64, 1024, 2048], P('sp', 'tp')
- proj_grad_t: float32 [2048, 512], P('sp', 'tp')
- input_grad: bfloat16 [12288, 512], P('sp', 'tp')
- branch_gate_grad: bfloat16 [12288, 512], P('sp', 'tp')
Inputs may be any that keep to these rules, and one draw needn't show every extreme that they name: `expert_ids`: each row names 2 different experts. Among the rows of one device no expert is named by more than 9 rows, a bound that some block reaches of some device.
All inputs are finite; a program needn't handle non-finite values.
Results may differ from a plain program's by a relative error of at most 0.023.
The roundings to bfloat16 on the way count: a program that leaves them out, or rounds other values in their place, can miss the bound.
Values may be sent and summed in bfloat16 or wider, within the bound.
A program may use at most 64 MiB of HBM per device.

v0:
```python
import jax
import jax.numpy as jnp
from jax import lax
from jax.sharding import PartitionSpec as P

RATE_SCALE = 8.0
CLAMP_LIMIT = 7.0
SHARPNESS = 1.702
NORM_EPSILON = 1e-06
STATE_FLOOR = 0.001
GELU_CUBIC = 0.044715
GELU_SCALE = 0.7978845608028654


def in_one_piece(arrays, axis, split_dim, concat_dim, along):
    ends, at = ([], 0)
    for a in arrays[:-1]:
        at += a.shape[along]
        ends.append(at)
    both = jnp.concatenate(arrays, axis=along)
    return tuple(
        jnp.split(
            lax.all_to_all(both, axis, split_axis=split_dim, concat_axis=concat_dim, tiled=True),
            ends,
            axis=along,
        )
    )


def side_by_side(arrays, axis, dim, along):
    widths = [a.shape[along] for a in arrays]
    both = jnp.concatenate(arrays, axis=along)
    out = lax.all_gather(both, axis, axis=dim, tiled=True)
    return tuple(jnp.split(out, [sum(widths[:k]) for k in range(1, len(widths))], axis=along))


def in_blocks(x, dim, count):
    dims = x.shape
    tiles = x.reshape(*dims[:dim], count, dims[dim] // count, *dims[dim + 1 :])
    return jnp.moveaxis(tiles, dim, 0)


def summed_on_arrival(x, axis, dim):
    tiles = in_blocks(x, dim, lax.axis_size(axis))
    arrived = lax.all_to_all(tiles, axis, split_axis=0, concat_axis=0, tiled=True)
    return arrived.astype(jnp.float32).sum(axis=0)


def laid_out(tiles, dim):
    tiles = jnp.moveaxis(tiles, 0, dim)
    dims = tiles.shape
    return tiles.reshape(*dims[:dim], dims[dim] * dims[dim + 1], *dims[dim + 2 :])


def sent_to_all(x, axis):
    copies = jnp.broadcast_to(x, (lax.axis_size(axis), *x.shape))
    return lax.all_to_all(copies, axis, split_axis=0, concat_axis=0, tiled=True)


def gathered_copies(x, axis, dim):
    return laid_out(sent_to_all(x, axis), dim)


def collected_together(x, axis):
    leaves = jax.tree.leaves(x)
    order = sorted(range(len(leaves)), key=lambda k: -leaves[k].size)
    width = (1, *leaves[order[0]].shape)[-1]
    lines = [
        jnp.pad(leaves[k].reshape(-1), (0, -leaves[k].size % width)).reshape(-1, width)
        for k in order
    ]
    both, at, found = (sent_to_all(jnp.concatenate(lines), axis), 0, {})
    for k, line in zip(order, lines):
        piece = both[:, at : at + len(line)].reshape(len(both), -1)
        found[k] = piece[:, : leaves[k].size].reshape(-1, *leaves[k].shape)
        at += len(line)
    numbers = iter(range(len(leaves)))
    return jax.tree.map(lambda _: found[next(numbers)], x)


def joined_by_halves(pieces, combine):
    while len(jax.tree.leaves(pieces)[0]) > 1:
        pieces = jax.vmap(combine)(
            *(jax.tree.map(lambda part: part[side::2], pieces) for side in (0, 1))
        )
    return jax.tree.map(lambda part: part[0], pieces)


def entering(x, axis, combine, identity, reverse):
    count, place = (lax.axis_size(axis), lax.axis_index(axis))
    passed = jnp.arange(count) > place if reverse else jnp.arange(count) < place

    def kept(part, zero, own):
        part = jnp.where(
            passed.reshape(-1, *(1 for _ in own.shape)), part, jnp.asarray(zero, own.dtype)
        )
        return part[::-1] if reverse else part

    pieces = collected_together(x, axis)
    return joined_by_halves(jax.tree.map(kept, pieces, identity, x), combine)


def shortened(x):
    return jax.tree.map(lambda a: a.astype(jnp.bfloat16) if a.dtype == jnp.float32 else a, x)


def with_halo(block, sides, width):
    for axis, dim in sides:
        count = lax.axis_size(axis)
        forward = [(i, i + 1) for i in range(count - 1)]
        backward = [(target, source) for source, target in forward]
        low = lax.ppermute(
            lax.slice_in_dim(block, block.shape[dim] - width, None, axis=dim), axis, forward
        )
        high = lax.ppermute(lax.slice_in_dim(block, 0, width, axis=dim), axis, backward)
        block = jnp.concatenate([low, block, high], axis=dim)
    return block


def gelu_parts(values):
    inside = GELU_SCALE * (values + GELU_CUBIC * values * values * values)
    tangent = jnp.tanh(inside)
    result = 0.5 * values * (1.0 + tangent)
    slope_value = 0.5 * (1.0 + tangent) + 0.5 * values * (1.0 - tangent * tangent) * GELU_SCALE * (
        1.0 + 3.0 * GELU_CUBIC * values * values
    )
    return (result, slope_value)


def chain_scan(factors, seeds):

    def link_pairs(first_pair, second_pair):
        return (first_pair[0] * second_pair[0], second_pair[0] * first_pair[1] + second_pair[1])

    return lax.associative_scan(link_pairs, (factors, seeds), axis=0)


def compose(former, latter):
    return (latter[0] * former[0], latter[0] * former[1] + latter[1])


def on_device(
    mid,
    out_grad,
    expert_ids,
    route_weights,
    gate_proj,
    up_proj,
    down_proj,
    out_proj,
    branch_gate,
    conv_out,
    prior_state,
    rate_gate_w,
    input_gate_w,
    decay_param,
    decay_jump,
    conv_taps,
):
    tok_rows, embedding_width = mid.shape
    shards = lax.axis_size("sp")
    groups = lax.axis_size("tp")
    local_experts = gate_proj.shape[0]
    experts_all = local_experts * shards
    top_count = expert_ids.shape[1]
    expert_room = 3 * top_count * tok_rows // (2 * experts_all)
    slot_count = experts_all * expert_room
    mid_full = mid.astype(jnp.float32)
    inv_rms = lax.rsqrt(jnp.mean(mid_full * mid_full, axis=1, keepdims=True) + NORM_EPSILON)
    normed = mid_full * inv_rms
    normed_b = normed.astype(jnp.bfloat16)
    flat_ids = expert_ids.reshape(-1)
    onehot = (flat_ids[:, None] == jnp.arange(experts_all, dtype=jnp.int32)[None, :]).astype(
        jnp.int32
    )
    rank_ids = jnp.sum((jnp.cumsum(onehot, axis=0) - onehot) * onehot, axis=1)
    slot_ids = (flat_ids * expert_room + rank_ids).reshape(tok_rows, top_count)
    matches = slot_ids[None, :, :] == jnp.arange(slot_count, dtype=jnp.int32)[:, None, None]
    select = jnp.any(matches, axis=2).astype(jnp.bfloat16)
    slot_gate = jnp.sum(jnp.where(matches, route_weights[None, :, :], 0.0), axis=(1, 2))
    column_span = embedding_width // groups
    offset = lax.axis_index("tp") * column_span
    rows_source = lax.dynamic_slice_in_dim(normed_b, offset, column_span, 1)
    grad_source = lax.dynamic_slice_in_dim(out_grad, offset, column_span, 1)
    sent_rows = jnp.dot(select, rows_source, preferred_element_type=jnp.float32).astype(
        jnp.bfloat16
    )
    dispatched_cotangent = (
        jnp.dot(select, grad_source, preferred_element_type=jnp.float32) * slot_gate[:, None]
    ).astype(jnp.bfloat16)
    got_rows, got_grad = in_one_piece((sent_rows, dispatched_cotangent), "sp", 0, 0, 1)
    got_rows, got_grad = side_by_side((got_rows, got_grad), "tp", 1, 0)
    expert_rows = jnp.swapaxes(
        got_rows.reshape(shards, local_experts, expert_room, embedding_width), 0, 1
    ).reshape(local_experts, shards * expert_room, embedding_width)
    expert_grads = jnp.swapaxes(
        got_grad.reshape(shards, local_experts, expert_room, embedding_width), 0, 1
    ).reshape(local_experts, shards * expert_room, embedding_width)
    gate_pre = jnp.einsum(
        "erd,edf->erf", expert_rows, gate_proj, preferred_element_type=jnp.float32
    )
    up_pre = jnp.einsum("erd,edf->erf", expert_rows, up_proj, preferred_element_type=jnp.float32)
    gate_clamped = jnp.minimum(gate_pre, CLAMP_LIMIT)
    up_clamped = jnp.clip(up_pre, -CLAMP_LIMIT, CLAMP_LIMIT)
    gate_sigmoid = jax.nn.sigmoid(SHARPNESS * gate_clamped)
    swish_value = gate_clamped * gate_sigmoid
    act_b = ((up_clamped + 1.0) * swish_value).astype(jnp.bfloat16)
    act_grad = jnp.einsum(
        "erd,efd->erf", expert_grads, down_proj, preferred_element_type=jnp.float32
    )
    gate_delta = jnp.where(
        gate_pre < CLAMP_LIMIT,
        act_grad
        * (up_clamped + 1.0)
        * (gate_sigmoid + SHARPNESS * swish_value * (1.0 - gate_sigmoid)),
        0.0,
    ).astype(jnp.bfloat16)
    up_delta = jnp.where(jnp.abs(up_pre) < CLAMP_LIMIT, act_grad * swish_value, 0.0).astype(
        jnp.bfloat16
    )
    down_grad = jnp.einsum(
        "erf,erd->efd", act_b, expert_grads, preferred_element_type=jnp.float32
    ).astype(jnp.bfloat16)
    gate_grad = jnp.einsum(
        "erd,erf->edf", expert_rows, gate_delta, preferred_element_type=jnp.float32
    ).astype(jnp.bfloat16)
    up_grad = jnp.einsum(
        "erd,erf->edf", expert_rows, up_delta, preferred_element_type=jnp.float32
    ).astype(jnp.bfloat16)
    partial_value = jnp.einsum(
        "erf,edf->erd", gate_delta, gate_proj, preferred_element_type=jnp.float32
    )
    partial_value = partial_value + jnp.einsum(
        "erf,edf->erd", up_delta, up_proj, preferred_element_type=jnp.float32
    )
    partial_rows = jnp.swapaxes(
        partial_value.reshape(local_experts, shards, expert_room, embedding_width), 0, 1
    ).reshape(slot_count, embedding_width)
    summed = summed_on_arrival(partial_rows.astype(jnp.bfloat16), "tp", 1)
    returned = lax.all_to_all(
        summed.astype(jnp.bfloat16), "sp", split_axis=0, concat_axis=0, tiled=True
    )
    token_grad = jnp.einsum("st,sd->td", select, returned, preferred_element_type=jnp.float32)
    token_grad = gathered_copies(token_grad.astype(jnp.bfloat16), "tp", 1).astype(token_grad.dtype)
    inner_mean = jnp.mean(token_grad * normed, axis=1, keepdims=True)
    mid_grad_b = (
        out_grad.astype(jnp.float32) + inv_rms * (token_grad - normed * inner_mean)
    ).astype(jnp.bfloat16)
    heads_local = rate_gate_w.shape[1]
    head_width = rate_gate_w.shape[2]
    channels = heads_local * head_width
    branch_grad = jnp.einsum("td,cd->tc", mid_grad_b, out_proj, preferred_element_type=jnp.float32)
    conv_heads = conv_out.reshape(2, tok_rows, heads_local, head_width)
    rate_gate = jax.nn.sigmoid(
        jnp.einsum(
            "sthc,shcd->sthd", conv_heads, rate_gate_w, preferred_element_type=jnp.float32
        ).reshape(2, tok_rows, channels)
    )
    input_gate = jax.nn.sigmoid(
        jnp.einsum(
            "sthc,shcd->sthd", conv_heads, input_gate_w, preferred_element_type=jnp.float32
        ).reshape(2, tok_rows, channels)
    )
    decay_rate = jax.nn.softplus(-decay_param)[:, None, :]
    log_decay = -RATE_SCALE * rate_gate * decay_rate + decay_jump
    decay_factors = jnp.exp(log_decay)
    squared = jnp.exp(2.0 * log_decay)
    norm_factor = jnp.sqrt(STATE_FLOOR - jnp.expm1(2.0 * log_decay))
    conv_full = conv_out.astype(jnp.float32)
    drive_term = input_gate * conv_full
    states = decay_factors * prior_state + norm_factor * drive_term
    summed_states = states[0] + states[1]
    gelu_value, gelu_slope = gelu_parts(branch_gate.astype(jnp.float32))
    mixed_b = (summed_states * gelu_value).astype(jnp.bfloat16)
    branch_gate_grad = (branch_grad * summed_states * gelu_slope).astype(jnp.bfloat16)
    state_grad = branch_grad * gelu_value
    ones_row = jnp.ones((1, channels), jnp.float32)
    later_factors = jnp.concatenate([decay_factors[0, 1:], ones_row], axis=0)
    later_prod, later_local = chain_scan(jnp.flip(later_factors, 0), jnp.flip(state_grad, 0))
    later_prod = jnp.flip(later_prod, 0)
    later_local = jnp.flip(later_local, 0)
    earlier_factors = jnp.concatenate([ones_row, decay_factors[1, :-1]], axis=0)
    earlier_prod, earlier_local = chain_scan(earlier_factors, state_grad)
    later_map = (decay_factors[0, 0] * later_prod[0], decay_factors[0, 0] * later_local[0])
    earlier_map = (
        decay_factors[1, -1] * earlier_prod[-1],
        decay_factors[1, -1] * earlier_local[-1],
    )
    identity = (jnp.ones((channels,), jnp.float32), jnp.zeros((channels,), jnp.float32))
    inflow_later = entering(later_map, "sp", compose, identity, True)[1]
    inflow_earlier = entering(earlier_map, "sp", compose, identity, False)[1]
    adjoint = jnp.stack(
        [
            later_local + later_prod * inflow_later[None, :],
            earlier_local + earlier_prod * inflow_earlier[None, :],
        ]
    )
    decay_grad = adjoint * (decay_factors * prior_state - drive_term * squared / norm_factor)
    drive_grad = adjoint * norm_factor
    rate_pre = (decay_grad * (-RATE_SCALE * decay_rate) * rate_gate * (1.0 - rate_gate)).astype(
        jnp.bfloat16
    )
    input_pre = (drive_grad * conv_full * input_gate * (1.0 - input_gate)).astype(jnp.bfloat16)
    conv_grad = drive_grad * input_gate
    conv_grad = conv_grad + jnp.einsum(
        "sthd,shcd->sthc",
        rate_pre.reshape(2, tok_rows, heads_local, head_width),
        rate_gate_w,
        preferred_element_type=jnp.float32,
    ).reshape(2, tok_rows, channels)
    conv_grad = conv_grad + jnp.einsum(
        "sthd,shcd->sthc",
        input_pre.reshape(2, tok_rows, heads_local, head_width),
        input_gate_w,
        preferred_element_type=jnp.float32,
    ).reshape(2, tok_rows, channels)
    reach = conv_taps.shape[1] - 1
    padded = with_halo(shortened(conv_grad), (("sp", 1),), reach).astype(conv_grad.dtype)
    taps_full = conv_taps.astype(jnp.float32)
    input_grad = jnp.zeros((tok_rows, channels), jnp.float32)
    for tap_index in range(reach + 1):
        upper = 2 * reach - tap_index
        input_grad = (
            input_grad
            + taps_full[0, tap_index] * padded[0, upper : upper + tok_rows]
            + taps_full[1, tap_index] * padded[1, tap_index : tap_index + tok_rows]
        )
    proj_grad_t = summed_on_arrival(
        jnp.einsum("td,tc->dc", mid_grad_b, mixed_b, preferred_element_type=jnp.float32).astype(
            jnp.bfloat16
        ),
        "sp",
        0,
    )
    return (
        gate_grad,
        up_grad,
        down_grad,
        proj_grad_t,
        input_grad.astype(jnp.bfloat16),
        branch_gate_grad,
    )


def solution(mesh):
    in_specs = (
        P("sp", None),
        P("sp", None),
        P("sp", None),
        P("sp", None),
        P("sp", None, "tp"),
        P("sp", None, "tp"),
        P("sp", "tp", None),
        P("tp", None),
        P("sp", "tp"),
        P(None, "sp", "tp"),
        P(None, "sp", "tp"),
        P(None, "tp", None, None),
        P(None, "tp", None, None),
        P(None, "tp"),
        P(None, "sp", "tp"),
        P(None, None, "tp"),
    )
    out_specs = (
        P("sp", None, "tp"),
        P("sp", None, "tp"),
        P("sp", "tp", None),
        P("sp", "tp"),
        P("sp", "tp"),
        P("sp", "tp"),
    )
    return jax.shard_map(
        on_device, mesh=mesh, in_specs=in_specs, out_specs=out_specs, check_vma=False
    )
```

profile of v0, /device:TPU:1, one launch (start us, length us, event | category | flops | bytes accessed | tf_op | source)
XLA Modules:
  0.0 322.6 jit_solution(7066043297634549402)
XLA Ops:
  16.8 62.8 %all_to_all.49 = bf16[64,9,1024]{2,1,0:T(8,128)(2,1)} all-to-all(bf16[64,9,1024]{2,1,0:T(8,128)(2,1)} %all_to_all.31), channel_id=1, replica_groups=mesh['sp'=64,'tp'=4] {'sp'}, dimensions={0} | all-to-all | bytes 2359296 | tf_op jit(solution)/shard_map/all_to_all | solution.py:23
  79.5 2.5 all_to_all.33
  83.3 52.9 %all-gather.2.cloned.1.call-done = bf16[1152,2048]{1,0:T(8,128)(2,1)} async-done(((bf16[1152,512]{1,0:T(8,128)(2,1)}), bf16[1152,2048]{1,0:T(8,128)(2,1)}) %all-gather.2.cloned.1.call-update) | async-done | bytes 4718608 | tf_op jit(solution)/shard_map/all_gather | solution.py:33
  136.2 2.6 fusion.9
  145.2 4.6 %all-to-all-start.1 = ((bf16[4,576,512]{2,1,0:T(8,128)(2,1)}), bf16[4,576,512]{2,1,0:T(8,128)(2,1)}, u32[]{:S(2)}, u32[]{:S(2)}) async-start(bf16[4,576,512]{2,1,0:T(8,128)(2,1)} %bitcast.208), calls=%async_computation.1 | async-start | bytes 4718592 | tf_op jit(solution)/shard_map/all_to_all | solution.py:45
  150.6 27.7 %all-to-all-done.1 = bf16[4,576,512]{2,1,0:T(8,128)(2,1)} async-done(((bf16[4,576,512]{2,1,0:T(8,128)(2,1)}), bf16[4,576,512]{2,1,0:T(8,128)(2,1)}, u32[]{:S(2)}, u32[]{:S(2)}) %all-to-all-start.1) | async-done | bytes 2359328 | tf_op jit(solution)/shard_map/all_to_all | solution.py:45
  178.3 2.3 reduce_sum.63
  181.8 11.7 %all-to-all-start.2 = ((bf16[64,9,512]{2,1,0:T(8,128)(2,1)}), bf16[64,9,512]{2,1,0:T(8,128)(2,1)S(1)}, u32[]{:S(2)}, u32[]{:S(2)}) async-start(bf16[64,9,512]{2,1,0:T(8,128)(2,1)} %all_to_all.35), calls=%async_computation.2 | async-start | bytes 2097152 | tf_op jit(solution)/shard_map/all_to_all | solution.py:240
  199.7 1.9 fusion.16
  203.9 17.8 %all-to-all-done.2 = bf16[64,9,512]{2,1,0:T(8,128)(2,1)S(1)} async-done(((bf16[64,9,512]{2,1,0:T(8,128)(2,1)}), bf16[64,9,512]{2,1,0:T(8,128)(2,1)S(1)}, u32[]{:S(2)}, u32[]{:S(2)}) %all-to-all-start.2) | async-done | bytes 589856 | tf_op jit(solution)/shard_map/all_to_all | solution.py:240
  225.2 3.7 %all-to-all-start.3 = ((bf16[4,192,512]{2,1,0:T(8,128)(2,1)}), bf16[4,192,512]{2,1,0:T(8,128)(2,1)S(1)}, u32[]{:S(2)}, u32[]{:S(2)}) async-start(bf16[4,192,512]{2,1,0:T(8,128)(2,1)} %broadcast_in_dim.67), calls=%async_computation.3 | async-start | bytes 1572864 | tf_op jit(solution)/shard_map/all_to_all | solution.py:57
  228.9 3.8 %fusion = bf16[1,2048,256]{2,1,0:T(8,128)(2,1)} fusion(bf16[576,256]{1,0:T(8,128)(2,1)} %copy-done.3, bf16[1152,2048]{1,0:T(8,128)(2,1)} %all-gather.2.cloned.1.call-done), kind=kOutput, calls=%fused_computation.4 | convolution fusion | flops 604504064 | bytes 3702784 | tf_op jit(solution)/shard_map/erd,erf->edf/dot_general | solution.py:224
  232.7 3.8 %fusion.2 = bf16[1,256,2048]{2,1,0:T(8,128)(2,1)} fusion(bf16[1152,2048]{1,0:T(8,128)(2,1)} %all-gather.2.cloned.1.call-done, f32[576,256]{1,0:T(8,128)S(1)} %copy-done.37, f32[576,256]{1,0:T(8,128)S(1)} %copy-done.39), kind=kOutput, calls=%fused_computation.6 | convolution fusion | flops 605978624 | bytes 4587520 | tf_op jit(solution)/shard_map/erf,erd->efd/dot_general | solution.py:221
  236.4 3.4 %all-to-all-done.3 = bf16[4,192,512]{2,1,0:T(8,128)(2,1)S(1)} async-done(((bf16[4,192,512]{2,1,0:T(8,128)(2,1)}), bf16[4,192,512]{2,1,0:T(8,128)(2,1)S(1)}, u32[]{:S(2)}, u32[]{:S(2)}) %all-to-all-start.3) | async-done | bytes 786464 | tf_op jit(solution)/shard_map/all_to_all | solution.py:57
  254.8 7.4 %all-to-all-start.6 = ((f32[64,2,128]{2,1,0:T(2,128)}), f32[64,2,128]{2,1,0:T(2,128)S(1)}, u32[]{:S(2)}, u32[]{:S(2)}) async-start(f32[64,2,128]{2,1,0:T(2,128)} %broadcast_in_dim.73), calls=%async_computation.6 | async-start | bytes 131072 | tf_op jit(solution)/shard_map/all_to_all | solution.py:57
  262.2 3.7 %fusion.1 = bf16[1,2048,256]{2,1,0:T(8,128)(2,1)} fusion(bf16[576,256]{1,0:T(8,128)(2,1)} %copy-done.13, bf16[1152,2048]{1,0:T(8,128)(2,1)} %all-gather.2.cloned.1.call-done), kind=kOutput, calls=%fused_computation.5 | convolution fusion | flops 604504064 | bytes 3702784 | tf_op jit(solution)/shard_map/erd,erf->edf/dot_general | solution.py:227
  267.0 5.2 %all-to-all-done.6 = f32[64,2,128]{2,1,0:T(2,128)S(1)} async-done(((f32[64,2,128]{2,1,0:T(2,128)}), f32[64,2,128]{2,1,0:T(2,128)S(1)}, u32[]{:S(2)}, u32[]{:S(2)}) %all-to-all-start.6) | async-done | bytes 65568 | tf_op jit(solution)/shard_map/all_to_all | solution.py:57
  272.9 5.1 %all-to-all-start.5 = ((f32[64,2,128]{2,1,0:T(2,128)}), f32[64,2,128]{2,1,0:T(2,128)S(1)}, u32[]{:S(2)}, u32[]{:S(2)}) async-start(f32[64,2,128]{2,1,0:T(2,128)} %broadcast_in_dim.69), calls=%async_computation.5 | async-start | bytes 131072 | tf_op jit(solution)/shard_map/all_to_all | solution.py:57
  279.1 9.0 %all-to-all-done.5 = f32[64,2,128]{2,1,0:T(2,128)S(1)} async-done(((f32[64,2,128]{2,1,0:T(2,128)}), f32[64,2,128]{2,1,0:T(2,128)S(1)}, u32[]{:S(2)}, u32[]{:S(2)}) %all-to-all-start.5) | async-done | bytes 65568 | tf_op jit(solution)/shard_map/all_to_all | solution.py:57
  289.4 1.9 multiply_convert_fusion.2
  292.6 4.6 %all-to-all-start.4 = ((bf16[64,32,128]{2,1,0:T(8,128)(2,1)}), bf16[64,32,128]{2,1,0:T(8,128)(2,1)S(1)}, u32[]{:S(2)}, u32[]{:S(2)}) async-start(bf16[64,32,128]{2,1,0:T(8,128)(2,1)} %bitcast.15), calls=%async_computation.4 | async-start | bytes 1048576 | tf_op jit(solution)/shard_map/all_to_all | solution.py:45
  300.0 2.5 collective-permute-start.1
  302.4 3.1 collective-permute-start
  307.0 8.0 %all-to-all-done.4 = bf16[64,32,128]{2,1,0:T(8,128)(2,1)S(1)} async-done(((bf16[64,32,128]{2,1,0:T(8,128)(2,1)}), bf16[64,32,128]{2,1,0:T(8,128)(2,1)S(1)}, u32[]{:S(2)}, u32[]{:S(2)}) %all-to-all-start.4) | async-done | bytes 524320 | tf_op jit(solution)/shard_map/all_to_all | solution.py:45
  (442 shorter events, 54.5 us)
Async XLA Ops:
  7.2 131.7 %copy-start = (bf16[1,2048,256]{2,1,0:T(8,128)(2,1)S(1)}, bf16[1,2048,256]{2,1,0:T(8,128)(2,1)}, u32[]{:S(2)}) copy-start(bf16[1,2048,256]{2,1,0:T(8,128)(2,1)} %param.20) | copy-start | bytes 3145732
  7.2 6.0 %copy-start.1 = (bf16[192,2048]{1,0:T(8,128)(2,1)S(1)}, bf16[192,2048]{1,0:T(8,128)(2,1)}, u32[]{:S(2)}) copy-start(bf16[192,2048]{1,0:T(8,128)(2,1)} %param.16) | copy-start | bytes 2359300
  7.2 129.0 %all-gather.2.cloned.1.call-start = ((), (), s32[]{:S(2)}) async-start(), calls=%async_computation.7 | async-start | bytes 5898240 | tf_op jit(solution)/shard_map/all_gather | solution.py:33
  82.2 54.0 %copy-start.2 = (bf16[1,2048,256]{2,1,0:T(8,128)(2,1)S(1)}, bf16[1,2048,256]{2,1,0:T(8,128)(2,1)}, u32[]{:S(2)}) copy-start(bf16[1,2048,256]{2,1,0:T(8,128)(2,1)} %param.21) | copy-start | bytes 3145732
  145.2 4.6 %copy-start.9 = (bf16[2,192,128]{2,1,0:T(8,128)(2,1)S(1)}, bf16[2,192,128]{2,1,0:T(8,128)(2,1)}, u32[]{:S(2)}) copy-start(bf16[2,192,128]{2,1,0:T(8,128)(2,1)} %param.25) | copy-start | bytes 294916
  145.2 4.8 %copy-start.20 = (bf16[2,2,64,64]{3,2,1,0:T(8,128)(2,1)S(1)}, bf16[2,2,64,64]{3,2,1,0:T(8,128)(2,1)}, u32[]{:S(2)}) copy-start(bf16[2,2,64,64]{3,2,1,0:T(8,128)(2,1)} %param.27) | copy-start | bytes 98308
  145.2 33.1 %all-to-all-start.1 = ((bf16[4,576,512]{2,1,0:T(8,128)(2,1)}), bf16[4,576,512]{2,1,0:T(8,128)(2,1)}, u32[]{:S(2)}, u32[]{:S(2)}) async-start(bf16[4,576,512]{2,1,0:T(8,128)(2,1)} %bitcast.208), calls=%async_computation.1 | async-start | bytes 4718592 | tf_op jit(solution)/shard_map/all_to_all | solution.py:45
  180.6 12.9 %copy-start.24 = (f32[2,128]{1,0:T(2,128)S(1)}, f32[2,128]{1,0:T(2,128)}, u32[]{:S(2)}) copy-start(f32[2,128]{1,0:T(2,128)} %param.29) | copy-start | bytes 3076
  180.6 12.9 %copy-start.18 = (f32[2,192,128]{2,1,0:T(8,128)S(1)}, f32[2,192,128]{2,1,0:T(8,128)}, u32[]{:S(2)}) copy-start(f32[2,192,128]{2,1,0:T(8,128)} %param.30) | copy-start | bytes 589828
  181.8 39.9 %all-to-all-start.2 = ((bf16[64,9,512]{2,1,0:T(8,128)(2,1)}), bf16[64,9,512]{2,1,0:T(8,128)(2,1)S(1)}, u32[]{:S(2)}, u32[]{:S(2)}) async-start(bf16[64,9,512]{2,1,0:T(8,128)(2,1)} %all_to_all.35), calls=%async_computation.2 | async-start | bytes 2097152 | tf_op jit(solution)/shard_map/all_to_all | solution.py:240
  193.5 9.2 %copy-start.23 = (bf16[2,4,128]{2,1,0:T(4,128)(2,1)S(1)}, bf16[2,4,128]{2,1,0:T(4,128)(2,1)}, u32[]{:S(2)}) copy-start(bf16[2,4,128]{2,1,0:T(4,128)(2,1)} %param.31) | copy-start | bytes 6148
  225.2 14.7 %all-to-all-start.3 = ((bf16[4,192,512]{2,1,0:T(8,128)(2,1)}), bf16[4,192,512]{2,1,0:T(8,128)(2,1)S(1)}, u32[]{:S(2)}, u32[]{:S(2)}) async-start(bf16[4,192,512]{2,1,0:T(8,128)(2,1)} %broadcast_in_dim.67), calls=%async_computation.3 | async-start | bytes 1572864 | tf_op jit(solution)/shard_map/all_to_all | solution.py:57
  228.9 3.8 %copy-start.37 = (f32[576,256]{1,0:T(8,128)S(1)}, f32[576,256]{1,0:T(8,128)}, u32[]{:S(2)}) copy-start(f32[576,256]{1,0:T(8,128)} %copy-done.36) | copy-start | bytes 1769476
  243.7 7.3 %copy-start.15 = (f32[95,128]{1,0:T(8,128)S(1)}, f32[95,128]{1,0:T(8,128)}, u32[]{:S(2)}) copy-start(f32[95,128]{1,0:T(8,128)} %slice.796) | copy-start | bytes 145924
  254.8 17.5 %all-to-all-start.6 = ((f32[64,2,128]{2,1,0:T(2,128)}), f32[64,2,128]{2,1,0:T(2,128)S(1)}, u32[]{:S(2)}, u32[]{:S(2)}) async-start(f32[64,2,128]{2,1,0:T(2,128)} %broadcast_in_dim.73), calls=%async_computation.6 | async-start | bytes 131072 | tf_op jit(solution)/shard_map/all_to_all | solution.py:57
  272.9 15.2 %all-to-all-start.5 = ((f32[64,2,128]{2,1,0:T(2,128)}), f32[64,2,128]{2,1,0:T(2,128)S(1)}, u32[]{:S(2)}, u32[]{:S(2)}) async-start(f32[64,2,128]{2,1,0:T(2,128)} %broadcast_in_dim.69), calls=%async_computation.5 | async-start | bytes 131072 | tf_op jit(solution)/shard_map/all_to_all | solution.py:57
  291.3 5.9 %copy-start.11 = (bf16[2,192,128]{2,1,0:T(8,128)(2,1)S(1)}, bf16[2,192,128]{2,1,0:T(8,128)(2,1)}, u32[]{:S(2)}) copy-start(bf16[2,192,128]{2,1,0:T(8,128)(2,1)} %get-tuple-element.22) | copy-start | bytes 294916
  292.6 5.9 %copy-start.10 = (bf16[2,192,128]{2,1,0:T(8,128)(2,1)S(1)}, bf16[2,192,128]{2,1,0:T(8,128)(2,1)}, u32[]{:S(2)}) copy-start(bf16[2,192,128]{2,1,0:T(8,128)(2,1)} %get-tuple-element.20) | copy-start | bytes 294916
  292.6 12.9 %copy-start.12 = (f32[192,128]{1,0:T(8,128)S(1)}, f32[192,128]{1,0:T(8,128)}, u32[]{:S(2)}) copy-start(f32[192,128]{1,0:T(8,128)} %get-tuple-element.126) | copy-start | bytes 294916
  292.6 22.4 %all-to-all-start.4 = ((bf16[64,32,128]{2,1,0:T(8,128)(2,1)}), bf16[64,32,128]{2,1,0:T(8,128)(2,1)S(1)}, u32[]{:S(2)}, u32[]{:S(2)}) async-start(bf16[64,32,128]{2,1,0:T(8,128)(2,1)} %bitcast.15), calls=%async_computation.4 | async-start | bytes 1048576 | tf_op jit(solution)/shard_map/all_to_all | solution.py:45
  297.2 9.1 %copy-start.21 = (f32[128]{0:T(128)S(1)}, f32[128]{0:T(128)}, u32[]{:S(2)}) copy-start(f32[128]{0:T(128)} %get-tuple-element.83) | copy-start | bytes 1540
  297.2 9.1 %copy-start.22 = (f32[128]{0:T(128)S(1)}, f32[128]{0:T(128)}, u32[]{:S(2)}) copy-start(f32[128]{0:T(128)} %get-tuple-element.84) | copy-start | bytes 1540
  300.0 6.3 %collective-permute-start.1 = (bf16[2,3,128]{2,1,0:T(4,128)(2,1)S(1)}, bf16[2,3,128]{2,1,0:T(4,128)(2,1)S(1)}, u32[]{:S(2)}, u32[]{:S(2)}) collective-permute-start(bf16[2,3,128]{2,1,0:T(4,128)(2,1)S(1)} %get-tuple-element.30), channel_id=1, source_target_pairs={{4,0},{8,4},{12,8},{16,12},{20,16},{24,20},{28,24},{32,28},{36,32}... | collective-permute-start | bytes 4616 | tf_op jit(solution)/shard_map/ppermute | solution.py:115
  302.4 3.8 %collective-permute-start = (bf16[2,3,128]{2,1,0:T(4,128)(2,1)S(1)}, bf16[2,3,128]{2,1,0:T(4,128)(2,1)S(1)}, u32[]{:S(2)}, u32[]{:S(2)}) collective-permute-start(bf16[2,3,128]{2,1,0:T(4,128)(2,1)S(1)} %get-tuple-element.29), channel_id=1, source_target_pairs={{0,4},{4,8},{8,12},{12,16},{16,20},{20,24},{24,28},{28,32},{32,36}... | collective-permute-start | bytes 4616 | tf_op jit(solution)/shard_map/ppermute | solution.py:112
  (25 other events, 36.0 us)
Sparse Core Ops, SparseCore 0:
  83.4 52.7 all-gather.1
where the time goes:
time: 324 us; the launch traced here: 323 us
  waiting for transfers between devices  124 us (38%)
  blocking collectives  62.8 us (19%)
  starting transfers between devices  42.6 us (13%)
  local copies, waits for them, and re-layouts  30.5 us (9%)
  matrix products  27 us (8%)
  other arithmetic  19.4 us (6%)
  between operations  16.1 us (5%)
    all_to_all x1, blocking collectives, in_one_piece(): lax.all_to_all(both, axis, split_axis=split_dim, concat_axis=concat_dim,...  62.8 us
    all_gather x1, waiting for transfers between devices, side_by_side(): out = lax.all_gather(both, axis, axis=dim, tiled=True)  52.9 us
    all_to_all x2, waiting for transfers between devices, summed_on_arrival(): lax.all_to_all(tiles, axis, split_axis=0, concat_axis=0, tiled=True)  35.7 us
    all_to_all x1, waiting for transfers between devices, on_device(): lax.all_to_all(summed.astype(jnp.bfloat16), 'sp', split_axis=0, concat_ax...  17.8 us
    all_to_all x3, waiting for transfers between devices, sent_to_all(): return lax.all_to_all(copies, axis, split_axis=0, concat_axis=0, tiled=True)  17.6 us
    all_to_all x3, starting transfers between devices, sent_to_all(): return lax.all_to_all(copies, axis, split_axis=0, concat_axis=0, tiled=True)  16.1 us
    all_to_all x1, starting transfers between devices, on_device(): lax.all_to_all(summed.astype(jnp.bfloat16), 'sp', split_axis=0, concat_ax...  11.7 us
    slice x97, local copies, waits for them, and re-layouts, chain_scan(): return lax.associative_scan(link_pairs, (factors, seeds), axis=0)  11 us
  transfers between devices with their start and end apart: 9, of which 7 were waited for; matrix products, arithmetic and copies ran while one was open for 9% of the time, Pallas kernels for 0%

commit v1 on v0

v1 whole, which is shorter than its diff:
```python
import functools
import math

import jax
import jax.numpy as jnp
from jax import lax
from jax.experimental import pallas as pl
from jax.experimental.pallas import tpu as pltpu
from jax.sharding import PartitionSpec as P

RATE_SCALE = 8.0
CLAMP_LIMIT = 7.0
SHARPNESS = 1.702
NORM_EPSILON = 1e-06
STATE_FLOOR = 0.001
GELU_CUBIC = 0.044715
GELU_SCALE = 0.7978845608028654

F32 = jnp.float32
BF16 = jnp.bfloat16
MESH = pl.DeviceIdType.MESH


def dot(a, b, ca=1, cb=0):
    return lax.dot_general(a, b, (((ca,), (cb,)), ((), ())), preferred_element_type=F32)


def gelu_parts(values):
    inside = GELU_SCALE * (values + GELU_CUBIC * values * values * values)
    tangent = jnp.tanh(inside)
    result = 0.5 * values * (1.0 + tangent)
    slope_value = 0.5 * (1.0 + tangent) + 0.5 * values * (1.0 - tangent * tangent) * GELU_SCALE * (
        1.0 + 3.0 * GELU_CUBIC * values * values
    )
    return (result, slope_value)


def less_one(x):
    series = jnp.ones_like(x)
    for n in range(8, 1, -1):
        series = 1.0 + x * (1.0 / n) * series
    return jnp.where(jnp.abs(x) < 0.35, x * series, jnp.exp(x) - 1.0)


class Sizes:
    def __init__(self, tok, d, ns, ny, room, ffl, ch):
        self.tok, self.d, self.ns, self.ny, self.room = tok, d, ns, ny, room
        self.ffl, self.ch = ffl, ch
        self.nj = math.isqrt(ns)
        self.nz = ns // self.nj
        self.bl = self.nj * room
        self.sl = ns * room
        self.hs = self.sl // 2
        self.ht = tok // 2
        self.nk = 2 * ny
        self.c = d // self.nk
        self.r = d // ns
        self.steps = [1 << i for i in range((tok - 1).bit_length())]


class Book:
    def __init__(self):
        self.n = 0

    def take(self, count):
        at, self.n = self.n, self.n + count
        return at


def layout(s):
    b = Book()
    return dict(
        s1=b.take(4 * s.nz), s2=b.take(4 * s.nj), y=b.take(16), rs=b.take(12),
        sa=b.take(2 * s.nj), sb=b.take(2 * s.nz), tg=b.take(8), cj=b.take(s.nj), cz=b.take(s.nz),
        halo=b.take(2), pj=b.take(s.nj), pz=b.take(s.nz),
    ), b.n


def kernel(s, *refs):
    (mid, og, idw, wg_hbm, wu_hbm, wd_hbm, outp, bgate, conv, prior, rgw, igw, dpar, djump, taps,
     gg_hbm, ug_hbm, dg_hbm, proj_out, ig_out, bgg_out,
     wgu, wd, inv_s, sel, gate, perm, s1, r1, s2, r2, xa, gu, ag, delta, act,
     p2, rt2, rb2, sp1, sm1, ft, fm, fo, rl, rr, s3, r3, s4, r4, tg, gg, ug, dg, mg,
     bd, gel, sslope, mixed, pst, prod, k1, k2, k3, dec, adj, cjs, cjr, czs, czr,
     cgr, hs_s, hr_s, pf, pr, ps2, pr2,
     ssem, rsem, lsem) = refs
    at, _ = layout(s)
    sp = lax.axis_index("sp")
    y = lax.axis_index("tp")
    z, j = sp // s.nj, sp % s.nj
    up, down = (y + 1) % s.ny, (y + s.ny - 1) % s.ny
    opp = (y + 2) % s.ny
    nxt, prv = (sp + 1) % s.ns, (sp + s.ns - 1) % s.ns

    def on_sp(i):
        return {"sp": i}

    def on_tp(i):
        return {"tp": i}

    def in_line(i):
        return {"sp": i * s.nj + j}

    def in_plane(i):
        return {"sp": z * s.nj + i}

    started = []

    def send(src, dst, si, ri, dev):
        cp = pltpu.make_async_remote_copy(
            src_ref=src, dst_ref=dst, send_sem=ssem.at[si], recv_sem=rsem.at[ri],
            device_id=dev, device_id_type=MESH)
        cp.start()
        started.append(cp)

    def recv(dst, ri):
        pltpu.make_async_remote_copy(
            src_ref=dst, dst_ref=dst, send_sem=ssem.at[0], recv_sem=rsem.at[ri],
            device_id=on_tp(up), device_id_type=MESH).wait_recv()

    def orders(n):
        half = n // 2
        out = [half]
        for d in range(half - 1, 0, -1):
            out += [d, n - d]
        return out if n > 2 else [1]

    loads = [
        pltpu.make_async_copy(wg_hbm, wgu.at[:, pl.ds(0, s.ffl)], lsem.at[0]),
        pltpu.make_async_copy(wu_hbm, wgu.at[:, pl.ds(s.ffl, s.ffl)], lsem.at[1]),
        pltpu.make_async_copy(wd_hbm, wd, lsem.at[2]),
    ]

    barrier = pltpu.get_barrier_semaphore()
    partners = [in_line((z + d) % s.nz) for d in range(1, s.nz)]
    partners += [in_plane((j + d) % s.nj) for d in range(1, s.nj)]
    partners += [on_tp(up), on_tp(down), on_sp(nxt), on_sp(prv)]
    for dev in partners:
        pl.semaphore_signal(barrier, inc=1, device_id=dev, device_id_type=MESH)
    for cp in loads:
        cp.start()

    squares = jnp.zeros((s.tok, s.c), F32)
    for k in range(s.nk):
        part = mid[:, k * s.c:(k + 1) * s.c].astype(F32)
        squares = squares + part * part
    inv = lax.rsqrt(jnp.sum(squares, axis=1, keepdims=True) * (1.0 / s.d) + NORM_EPSILON)
    inv_s[...] = jnp.broadcast_to(inv, inv_s.shape)
    ids0, ids1 = idw[0:1, :], idw[1:2, :]
    w0, w1 = idw[2:3, :], idw[3:4, :]
    names = lax.broadcasted_iota(jnp.int32, (s.ns, s.tok), 0).astype(F32)
    hit0, hit1 = names == ids0, names == ids1
    hits = jnp.where(hit0 | hit1, 1.0, 0.0)
    before = jnp.where(
        lax.broadcasted_iota(jnp.int32, (s.tok, s.tok), 0)
        < lax.broadcasted_iota(jnp.int32, (s.tok, s.tok), 1), 1.0, 0.0)
    counts = dot(hits.astype(BF16), before.astype(BF16))
    slot0 = ids0 * s.room + jnp.sum(jnp.where(hit0, counts, 0.0), axis=0, keepdims=True)
    slot1 = ids1 * s.room + jnp.sum(jnp.where(hit1, counts, 0.0), axis=0, keepdims=True)
    rows = lax.broadcasted_iota(jnp.int32, (s.sl, s.tok), 0).astype(F32)
    own0, own1 = rows == slot0, rows == slot1
    sel[...] = jnp.where(own0 | own1, 1.0, 0.0).astype(BF16)
    gate[...] = jnp.sum(jnp.where(own0, w0, 0.0) + jnp.where(own1, w1, 0.0), axis=1, keepdims=True)
    line = lax.broadcasted_iota(jnp.int32, (s.sl, 1), 0).astype(F32)
    outer = jnp.floor((line + 0.5) * (1.0 / s.bl))
    rest = line - outer * s.bl
    inner = jnp.floor((rest + 0.5) * (1.0 / s.room))
    source = inner * s.bl + outer * s.room + (rest - inner * s.room)
    perm[...] = jnp.where(
        lax.broadcasted_iota(jnp.int32, (s.sl, s.sl), 1).astype(F32) == source, 1.0, 0.0
    ).astype(BF16)

    def quarter(c):
        return pl.ds(pl.multiple_of((y * 2 + c) * s.c, s.c), s.c)

    def blocks(x):
        return x.reshape(-1, s.bl, s.c).astype(BF16)

    def flat(ref):
        return ref.astype(F32).reshape(s.sl, s.c).astype(BF16)

    for q in range(4):
        c, kind = q // 2, q % 2
        if kind == 0:
            piece = (mid[:, quarter(c)].astype(F32) * inv_s[:, 0:1]).astype(BF16)
            value = dot(sel[...], piece)
        else:
            value = dot(sel[...], og[:, quarter(c)]) * gate[...]
        s1[q] = blocks(value)
        if q == 0:
            pl.semaphore_wait(barrier, len(partners))
        for d in orders(s.nz):
            zd = (z + d) % s.nz
            send(s1.at[q, zd], r1.at[q, z], at["s1"] + q * s.nz + zd, at["s1"] + q * s.nz + z, in_line(zd))
        r1[q, z] = s1[q, z]

    for side in range(2):
        for n, w in enumerate((rgw, igw)):
            zero = jnp.zeros((w.shape[2], w.shape[3]), F32)
            top = jnp.concatenate([w[side, 0].astype(F32), zero], axis=1)
            low = jnp.concatenate([zero, w[side, 1].astype(F32)], axis=1)
            bd[2 * side + n] = jnp.concatenate([top, low], axis=0).astype(BF16)
    gelu_value, gelu_slope = gelu_parts(bgate[...].astype(F32))
    gel[...] = gelu_value
    both_states = jnp.zeros((s.tok, s.ch), F32)
    time = lax.broadcasted_iota(jnp.int32, (s.tok, s.ch), 0)
    for side in range(2):
        conv_b = conv[side]
        conv_f = conv_b.astype(F32)
        rate_gate = jax.nn.sigmoid(dot(conv_b, bd[2 * side]))
        input_gate = jax.nn.sigmoid(dot(conv_b, bd[2 * side + 1]))
        decay_rate = dpar[side:side + 1, :]
        log_decay = -RATE_SCALE * rate_gate * decay_rate + djump[side]
        factors = jnp.exp(log_decay)
        squared = jnp.exp(2.0 * log_decay)
        norm_factor = jnp.sqrt(STATE_FLOOR - less_one(2.0 * log_decay))
        drive = input_gate * conv_f
        carried = factors * prior[side]
        both_states = both_states + (carried + norm_factor * drive)
        k1[side] = (carried - drive * squared / norm_factor) * (
            -RATE_SCALE * decay_rate) * rate_gate * (1.0 - rate_gate)
        k2[side] = norm_factor * conv_f * input_gate * (1.0 - input_gate)
        k3[side] = norm_factor * input_gate
        if side == 0:
            link = jnp.where(time < s.tok - 1, pltpu.roll(factors, s.tok - 1, 0), 1.0)
            dec[0:1, :] = factors[0:1, :]
        else:
            link = jnp.where(time > 0, pltpu.roll(factors, 1, 0), 1.0)
            dec[1:2, :] = factors[s.tok - 1:s.tok, :]
        for n, d in enumerate(s.steps):
            inside = time < s.tok - d if side == 0 else time >= d
            pst[side, n] = jnp.where(inside, link, 0.0)
            shift = s.tok - d if side == 0 else d
            link = jnp.where(inside, link * pltpu.roll(link, shift, 0), link)
        prod[side] = link
    sslope[...] = both_states * gelu_slope
    mixed[...] = (both_states * gelu_value).astype(BF16)

    def turn(q):
        for d in range(1, s.nz):
            zs = (z + d) % s.nz
            recv(r1.at[q, zs], at["s1"] + q * s.nz + zs)
        s2[q] = blocks(dot(perm[...], flat(r1[q])))
        for d in orders(s.nj):
            jd = (j + d) % s.nj
            send(s2.at[q, jd], r2.at[q, j], at["s2"] + q * s.nj + jd, at["s2"] + q * s.nj + j, in_plane(jd))
        r2[q, j] = s2[q, j]

    top, low = pl.ds(0, s.hs), pl.ds(s.hs, s.hs)

    def spread(q):
        c, kind = q // 2, q % 2
        for d in range(1, s.nj):
            js = (j + d) % s.nj
            recv(r2.at[q, js], at["s2"] + q * s.nj + js)
        xa[kind, y * 2 + c] = flat(r2[q])
        ref = xa.at[kind, y * 2 + c]
        n = at["y"] + 4 * q
        send(ref, ref, n, n, on_tp(up))
        send(ref, ref, n + 1, n + 1, on_tp(down))

    def relay(q):
        c, kind = q // 2, q % 2
        n = at["y"] + 4 * q
        ref = xa.at[kind, down * 2 + c]
        recv(ref, n)
        send(ref.at[top], ref.at[top], n + 2, n + 2, on_tp(up))
        ref = xa.at[kind, up * 2 + c]
        recv(ref, n + 1)
        send(ref.at[low], ref.at[low], n + 3, n + 3, on_tp(down))

    def weights_of(k):
        return wgu[pl.ds(pl.multiple_of(k * s.c, s.c), s.c), :]

    def take(q):
        c, kind = q // 2, q % 2
        n = at["y"] + 4 * q
        far = xa.at[kind, opp * 2 + c]
        recv(far.at[top], n + 2)
        recv(far.at[low], n + 3)
        for i in range(s.ny):
            k = i * 2 + c
            if kind == 0:
                value = dot(xa[0, k], wgu[k * s.c:(k + 1) * s.c, :])
                total = gu
            else:
                value = dot(xa[1, k], wd[:, k * s.c:(k + 1) * s.c], 1, 1)
                total = ag
            if c == 0 and i == 0:
                total[...] = value
            else:
                total[...] += value

    turn(0)
    turn(1)
    spread(0)
    turn(2)
    spread(1)
    relay(0)
    turn(3)
    spread(2)
    relay(1)
    for cp in loads:
        cp.wait()
    take(0)
    spread(3)
    relay(2)
    take(1)
    relay(3)
    take(2)
    take(3)

    gate_pre, up_pre = gu[:, :s.ffl], gu[:, s.ffl:]
    act_grad = ag[...]
    gate_clamped = jnp.minimum(gate_pre, CLAMP_LIMIT)
    up_clamped = jnp.clip(up_pre, -CLAMP_LIMIT, CLAMP_LIMIT)
    gate_sigmoid = jax.nn.sigmoid(SHARPNESS * gate_clamped)
    swish_value = gate_clamped * gate_sigmoid
    act[...] = ((up_clamped + 1.0) * swish_value).astype(BF16)
    delta[:, :s.ffl] = jnp.where(
        gate_pre < CLAMP_LIMIT,
        act_grad * (up_clamped + 1.0)
        * (gate_sigmoid + SHARPNESS * swish_value * (1.0 - gate_sigmoid)), 0.0).astype(BF16)
    delta[:, s.ffl:] = jnp.where(
        jnp.abs(up_pre) < CLAMP_LIMIT, act_grad * swish_value, 0.0).astype(BF16)

    def partial(owner, c):
        return dot(delta[...], weights_of(owner * 2 + c), 1, 1)

    for c in range(2):
        n = at["rs"] + 6 * c
        p2[c] = partial(opp, c).astype(BF16)
        send(p2.at[c, top], rt2.at[c], n, n, on_tp(up))
        send(p2.at[c, low], rb2.at[c], n + 1, n + 1, on_tp(down))
    for c in range(2):
        n = at["rs"] + 6 * c
        value = partial(up, c)
        sp1[c, s.hs:, :] = value[s.hs:].astype(BF16)
        ft[c] = value[:s.hs]
        send(sp1.at[c, low], rl.at[c, low], n + 2, n + 2, on_tp(up))
        value = partial(down, c)
        sm1[c, :s.hs, :] = value[:s.hs].astype(BF16)
        fm[c] = value[s.hs:]
        send(sm1.at[c, top], rr.at[c, top], n + 3, n + 3, on_tp(down))

    def pass_on(c):
        n = at["rs"] + 6 * c
        recv(rt2.at[c], n)
        sp1[c, :s.hs, :] = (ft[c] + rt2[c].astype(F32)).astype(BF16)
        send(sp1.at[c, top], rl.at[c, top], n + 4, n + 4, on_tp(up))
        recv(rb2.at[c], n + 1)
        sm1[c, s.hs:, :] = (fm[c] + rb2[c].astype(F32)).astype(BF16)
        send(sm1.at[c, low], rr.at[c, low], n + 5, n + 5, on_tp(down))

    pass_on(0)
    for c in range(2):
        fo[c] = partial(y, c)
    pass_on(1)

    @pl.loop(0, s.nk)
    def _(k):
        value = dot(xa[0, k], delta[...], 0, 0)
        where = pl.ds(pl.multiple_of(k * s.c, s.c), s.c)
        gg[where, :] = value[:, :s.ffl].astype(BF16)
        ug[where, :] = value[:, s.ffl:].astype(BF16)

    stores = [
        pltpu.make_async_copy(gg, gg_hbm, lsem.at[3]),
        pltpu.make_async_copy(ug, ug_hbm, lsem.at[4]),
        pltpu.make_async_copy(dg, dg_hbm, lsem.at[5]),
    ]
    stores[0].start()
    stores[1].start()

    def give(c):
        n = at["rs"] + 6 * c
        recv(rl.at[c, low], n + 2)
        recv(rr.at[c, top], n + 3)
        recv(rl.at[c, top], n + 4)
        recv(rr.at[c, low], n + 5)
        s3[c] = blocks(fo[c] + rl[c].astype(F32) + rr[c].astype(F32))
        for d in orders(s.nj):
            jd = (j + d) % s.nj
            send(s3.at[c, jd], r3.at[c, j], at["sa"] + c * s.nj + jd, at["sa"] + c * s.nj + j, in_plane(jd))
        r3[c, j] = s3[c, j]

    def turn_back(c):
        for d in range(1, s.nj):
            js = (j + d) % s.nj
            recv(r3.at[c, js], at["sa"] + c * s.nj + js)
        s4[c] = blocks(dot(perm[...], flat(r3[c])))
        for d in orders(s.nz):
            zd = (z + d) % s.nz
            send(s4.at[c, zd], r4.at[c, z], at["sb"] + c * s.nz + zd, at["sb"] + c * s.nz + z, in_line(zd))
        r4[c, z] = s4[c, z]

    ttop, tlow = pl.ds(0, s.ht), pl.ds(s.ht, s.ht)

    def combine(c):
        for d in range(1, s.nz):
            zs = (z + d) % s.nz
            recv(r4.at[c, zs], at["sb"] + c * s.nz + zs)
        tg[y * 2 + c] = dot(sel[...], flat(r4[c]), 0, 0).astype(BF16)
        ref = tg.at[y * 2 + c]
        n = at["tg"] + 4 * c
        send(ref, ref, n, n, on_tp(up))
        send(ref, ref, n + 1, n + 1, on_tp(down))

    def tg_relay(c):
        n = at["tg"] + 4 * c
        ref = tg.at[down * 2 + c]
        recv(ref, n)
        send(ref.at[ttop], ref.at[ttop], n + 2, n + 2, on_tp(up))
        ref = tg.at[up * 2 + c]
        recv(ref, n + 1)
        send(ref.at[tlow], ref.at[tlow], n + 3, n + 3, on_tp(down))

    def tg_take(c):
        n = at["tg"] + 4 * c
        ref = tg.at[opp * 2 + c]
        recv(ref.at[ttop], n + 2)
        recv(ref.at[tlow], n + 3)

    give(0)
    give(1)
    turn_back(0)

    @pl.loop(0, s.nk)
    def _(k):
        value = dot(act[...], xa[1, k], 0, 0)
        dg[:, pl.ds(pl.multiple_of(k * s.c, s.c), s.c)] = value.astype(BF16)

    stores[2].start()
    turn_back(1)
    combine(0)
    tg_relay(0)
    combine(1)
    tg_take(0)
    tg_relay(1)
    tg_take(1)

    inv_col = inv_s[:, 0:1]
    prods = jnp.zeros((s.tok, s.c), F32)
    for k in range(s.nk):
        part = mid[:, k * s.c:(k + 1) * s.c].astype(F32) * inv_col
        prods = prods + tg[k].astype(F32) * part
    inner_mean = jnp.sum(prods, axis=1, keepdims=True) * (1.0 / s.d)
    branch_grad = jnp.zeros((s.tok, s.ch), F32)
    for k in range(s.nk):
        cols = slice(k * s.c, (k + 1) * s.c)
        part = mid[:, cols].astype(F32) * inv_col
        value = (og[:, cols].astype(F32) + inv_col * (tg[k].astype(F32) - part * inner_mean)).astype(BF16)
        mg[k] = value
        branch_grad = branch_grad + dot(value, outp[:, cols], 1, 1)
    bgg_out[...] = (branch_grad * sslope[...]).astype(BF16)
    state_grad = branch_grad * gel[...]

    for side in range(2):
        chain = state_grad
        for n, d in enumerate(s.steps):
            shift = s.tok - d if side == 0 else d
            chain = chain + pst[side, n] * pltpu.roll(chain, shift, 0)
        adj[side] = chain
        edge = slice(0, 1) if side == 0 else slice(s.tok - 1, s.tok)
        cjs[2 * side:2 * side + 1, :] = dec[side:side + 1, :] * prod[side, edge, :]
        cjs[2 * side + 1:2 * side + 2, :] = dec[side:side + 1, :] * chain[edge]
    cjr[j] = cjs[...]
    for d in orders(s.nj):
        jd = (j + d) % s.nj
        send(cjs, cjr.at[j], at["cj"] + jd, at["cj"] + j, in_plane(jd))

    def project(k):
        value = dot(mg[k], mixed[...], 0, 0).astype(BF16)
        if s.c == s.nj * s.r:
            pf[k] = value.reshape(s.nj, s.r, s.ch)
        else:
            a = k * s.c
            pf[a // (s.nj * s.r), (a // s.r) % s.nj, pl.ds(a % s.r, s.c), :] = value

    for k in range(s.nk):
        project(k)
    for d in orders(s.nj):
        jd = (j + d) % s.nj
        send(pf.at[:, jd], pr.at[j], at["pj"] + jd, at["pj"] + j, in_plane(jd))
    pr[j] = pf[:, j]

    for d in range(1, s.nj):
        js = (j + d) % s.nj
        recv(cjr.at[js], at["cj"] + js)

    def compose(got, count, place):
        one, nil = jnp.ones((1, s.ch), F32), jnp.zeros((1, s.ch), F32)
        later, earlier = (one, nil), (one, nil)
        whole_l, whole_e = (one, nil), (one, nil)
        for i in range(count - 1, -1, -1):
            a, b = got[i, 0:1, :], got[i, 1:2, :]
            whole_l = (whole_l[0] * a, a * whole_l[1] + b)
            keep = i > place
            later = (jnp.where(keep, whole_l[0], later[0]), jnp.where(keep, whole_l[1], later[1]))
        for i in range(count):
            a, b = got[i, 2:3, :], got[i, 3:4, :]
            whole_e = (whole_e[0] * a, a * whole_e[1] + b)
            keep = i < place
            earlier = (jnp.where(keep, whole_e[0], earlier[0]), jnp.where(keep, whole_e[1], earlier[1]))
        return later, earlier, whole_l, whole_e

    later_j, earlier_j, whole_l, whole_e = compose(cjr, s.nj, j)
    czs[0:1, :], czs[1:2, :] = whole_l
    czs[2:3, :], czs[3:4, :] = whole_e
    czr[z] = czs[...]
    for d in orders(s.nz):
        zd = (z + d) % s.nz
        send(czs, czr.at[z], at["cz"] + zd, at["cz"] + z, in_line(zd))

    for d in range(1, s.nj):
        js = (j + d) % s.nj
        recv(pr.at[js], at["pj"] + js)
    total = pr[0].astype(F32)
    for i in range(1, s.nj):
        total = total + pr[i].astype(F32)
    ps2[...] = total.astype(BF16)
    pr2[z] = ps2[z]

    for d in range(1, s.nz):
        zs = (z + d) % s.nz
        recv(czr.at[zs], at["cz"] + zs)
    for d in orders(s.nz):
        zd = (z + d) % s.nz
        send(ps2.at[zd], pr2.at[z], at["pz"] + zd, at["pz"] + z, in_line(zd))
    later_z, earlier_z, _, _ = compose(czr, s.nz, z)
    inflow = (later_j[0] * later_z[1] + later_j[1], earlier_j[0] * earlier_z[1] + earlier_j[1])

    for side in range(2):
        adjoint = adj[side] + prod[side] * inflow[side]
        rate_pre = (adjoint * k1[side]).astype(BF16)
        input_pre = (adjoint * k2[side]).astype(BF16)
        cgr[side] = (adjoint * k3[side] + dot(rate_pre, bd[2 * side], 1, 1)
                     + dot(input_pre, bd[2 * side + 1], 1, 1))
    hs_s[0] = cgr[0, 0:8, :]
    hs_s[1] = cgr[1, s.tok - 8:s.tok, :]
    send(hs_s.at[0], hr_s.at[0], at["halo"], at["halo"], on_sp(prv))
    send(hs_s.at[1], hr_s.at[1], at["halo"] + 1, at["halo"] + 1, on_sp(nxt))
    recv(hr_s.at[0], at["halo"])
    recv(hr_s.at[1], at["halo"] + 1)
    after = jnp.where(sp < s.ns - 1, hr_s[0], 0.0)
    ahead = jnp.where(sp > 0, hr_s[1], 0.0)
    ext0 = jnp.concatenate([cgr[0], after], axis=0)
    ext1 = jnp.concatenate([ahead, cgr[1]], axis=0)
    reach = taps.shape[1] - 1
    tap = taps[...].astype(F32)
    result = jnp.zeros((s.tok, s.ch), F32)
    for t in range(reach + 1):
        off = reach - t
        result = (result + tap[0, t:t + 1, :] * ext0[off:off + s.tok]
                  + tap[1, t:t + 1, :] * ext1[8 - off:8 - off + s.tok])
    ig_out[...] = result.astype(BF16)

    for d in range(1, s.nz):
        zs = (z + d) % s.nz
        recv(pr2.at[zs], at["pz"] + zs)
    total = pr2[0].astype(F32)
    for i in range(1, s.nz):
        total = total + pr2[i].astype(F32)
    proj_out[...] = total

    for cp in stores:
        cp.wait()
    for cp in started:
        cp.wait_send()


def on_device(mid, out_grad, expert_ids, route_weights, gate_proj, up_proj, down_proj, out_proj,
              branch_gate, conv_out, prior_state, rate_gate_w, input_gate_w, decay_param,
              decay_jump, conv_taps):
    tok, d = mid.shape
    ns, ny = lax.axis_size("sp"), lax.axis_size("tp")
    room = 3 * expert_ids.shape[1] * tok // (2 * ns)
    ffl, ch = gate_proj.shape[2], out_proj.shape[0]
    s = Sizes(tok, d, ns, ny, room, ffl, ch)
    idw = jnp.concatenate([expert_ids.astype(F32).T, route_weights.T], axis=0)
    decay_rate = jax.nn.softplus(-decay_param)
    _, count = layout(s)
    vm, hbm = pl.BlockSpec(memory_space=pltpu.VMEM), pl.BlockSpec(memory_space=pl.ANY)
    nst = len(s.steps)

    def b(*shape):
        return pltpu.VMEM(shape, BF16)

    def f(*shape):
        return pltpu.VMEM(shape, F32)

    scratch = [
        b(d, 2 * ffl), b(ffl, d), f(tok, 128), b(s.sl, tok), f(s.sl, 1), b(s.sl, s.sl),
        b(4, s.nz, s.bl, s.c), b(4, s.nz, s.bl, s.c), b(4, s.nj, s.bl, s.c), b(4, s.nj, s.bl, s.c),
        b(2, s.nk, s.sl, s.c), f(s.sl, 2 * ffl), f(s.sl, ffl), b(s.sl, 2 * ffl), b(s.sl, ffl),
        b(2, s.sl, s.c), b(2, s.hs, s.c), b(2, s.hs, s.c), b(2, s.sl, s.c), b(2, s.sl, s.c),
        f(2, s.hs, s.c), f(2, s.hs, s.c), f(2, s.sl, s.c), b(2, s.sl, s.c), b(2, s.sl, s.c),
        b(2, s.nj, s.bl, s.c), b(2, s.nj, s.bl, s.c), b(2, s.nz, s.bl, s.c), b(2, s.nz, s.bl, s.c),
        b(s.nk, tok, s.c), b(d, ffl), b(d, ffl), b(ffl, d), b(s.nk, tok, s.c),
        b(4, ch, ch), f(tok, ch), f(tok, ch), b(tok, ch), f(2, nst, tok, ch), f(2, tok, ch),
        f(2, tok, ch), f(2, tok, ch), f(2, tok, ch), f(2, ch), f(2, tok, ch),
        f(4, ch), f(s.nj, 4, ch), f(4, ch), f(s.nz, 4, ch),
        f(2, tok, ch), f(2, 8, ch), f(2, 8, ch),
        b(s.nz, s.nj, s.r, ch), b(s.nj, s.nz, s.r, ch), b(s.nz, s.r, ch), b(s.nz, s.r, ch),
        pltpu.SemaphoreType.DMA((count,)), pltpu.SemaphoreType.DMA((count,)),
        pltpu.SemaphoreType.DMA((6,)),
    ]
    shape = jax.ShapeDtypeStruct
    outs = pl.pallas_call(
        functools.partial(kernel, s),
        out_shape=(shape((d, ffl), BF16), shape((d, ffl), BF16), shape((ffl, d), BF16),
                   shape((s.r, ch), F32), shape((tok, ch), BF16), shape((tok, ch), BF16)),
        in_specs=[vm, vm, vm, hbm, hbm, hbm] + [vm] * 9,
        out_specs=(hbm, hbm, hbm, vm, vm, vm),
        scratch_shapes=scratch,
        compiler_params=pltpu.CompilerParams(
            collective_id=0, has_side_effects=True, vmem_limit_bytes=60 * 1024 * 1024),
        name="step",
    )(mid, out_grad, idw, gate_proj[0], up_proj[0], down_proj[0], out_proj, branch_gate, conv_out,
      prior_state, rate_gate_w, input_gate_w, decay_rate, decay_jump, conv_taps)
    gg, ug, dg, proj, ig, bgg = outs
    return gg[None], ug[None], dg[None], proj, ig, bgg


def solution(mesh):
    in_specs = (
        P("sp", None), P("sp", None), P("sp", None), P("sp", None),
        P("sp", None, "tp"), P("sp", None, "tp"), P("sp", "tp", None), P("tp", None),
        P("sp", "tp"), P(None, "sp", "tp"), P(None, "sp", "tp"), P(None, "tp", None, None),
        P(None, "tp", None, None), P(None, "tp"), P(None, "sp", "tp"), P(None, None, "tp"),
    )
    out_specs = (
        P("sp", None, "tp"), P("sp", None, "tp"), P("sp", "tp", None),
        P("sp", "tp"), P("sp", "tp"), P("sp", "tp"),
    )
    return jax.shard_map(
        on_device, mesh=mesh, in_specs=in_specs, out_specs=out_specs, check_vma=False
    )
```

time: 324 us -> 143 us (0.44)
  Pallas kernels: 0 us -> 131 us
  waiting for transfers between devices: 124 us -> 0 us
  blocking collectives: 62.8 us -> 0 us
  starting transfers between devices: 42.6 us -> 0 us
  matrix products: 27 us -> 0 us
  local copies, waits for them, and re-layouts: 30.5 us -> 8.32 us
  other arithmetic: 19.4 us -> 1.18 us
  between operations: 16.1 us -> 0.68 us
    pallas_call x0 -> x1, Pallas kernels: none -> 131 us  [on_device(): pl.pallas_call(functools.partial(kernel, s), out_shape=(shape((d, ffl), B...]
    all_to_all x6 -> x0, waiting for transfers between devices: 71.2 us -> none  [the longest x2 35.7 us: summed_on_arrival(): lax.all_to_all(tiles, axis, split_axis=0, concat_axis=0, tiled=True)]
    all_to_all x1 -> x0, blocking collectives: 62.8 us -> none  [in_one_piece(): lax.all_to_all(both, axis, split_axis=split_dim, concat_axis=concat_dim,...]
    all_gather x1 -> x0, waiting for transfers between devices: 52.9 us -> none  [side_by_side(): out = lax.all_gather(both, axis, axis=dim, tiled=True)]
    all_to_all x6 -> x0, starting transfers between devices: 37 us -> none  [the longest x3 16.1 us: sent_to_all(): return lax.all_to_all(copies, axis, split_axis=0, concat_axis=0, tiled=True)]
    dot_general x17 -> x0, matrix products: 27 us -> none  [the longest x1 3.79 us: on_device(): jnp.einsum('erd,erf->edf', expert_rows, gate_delta, preferred_element_typ...]
    slice x145 -> x0, local copies, waits for them, and re-layouts: 11.9 us -> none  [the longest x97 11 us: chain_scan(): return lax.associative_scan(link_pairs, (factors, seeds), axis=0)]
    all_to_all x4 -> x0, local copies, waits for them, and re-layouts: 6.38 us -> none  [the longest x2 4.11 us: in_one_piece(): lax.all_to_all(both, axis, split_axis=split_dim, concat_axis=concat_dim,...]
  transfers between devices with their start and end apart: 9 -> 0, of which waited for: 7 -> 0; matrix products, arithmetic and copies ran while one was open for 9% -> 0% of each run, Pallas kernels for 0% -> 0%
where the time goes in v1:
time: 143 us; the launch traced here: 142 us
  Pallas kernels  131 us (92%)
  local copies, waits for them, and re-layouts  8.32 us (6%)
    pallas_call x1, Pallas kernels, on_device(): pl.pallas_call(functools.partial(kernel, s), out_shape=(shape((d, ffl), B...  131 us
    unnamed x22, local copies, waits for them, and re-layouts  8.32 us

profile of v1, /device:TPU:1, one launch (start us, length us, event | category | flops | bytes accessed | tf_op | source)
XLA Modules:
  0.0 141.6 jit_solution(18012196791444279043)
XLA Ops:
  0.6 0.0 copy-start.7
  0.6 0.0 copy-start.5
  0.7 0.7 copy-done.7
  1.3 0.6 compare_select_fusion.refs_12_
  1.9 0.0 copy-done.5
  1.9 0.0 copy-start.6
  1.9 0.7 copy-done.6
  2.6 0.6 pad_maximum_fusion.refs_2_
  3.2 131.4 %step.1 = (bf16[2048,256]{1,0:T(8,128)(2,1)}, bf16[2048,256]{1,0:T(8,128)(2,1)}, bf16[256,2048]{1,0:T(8,128)(2,1)}, f32[32,128]{1,0:T(8,128)}, bf16[192,128]{1,0:T(8,128)(2,1)}, /*index=5*/bf16[192,128]{1,0:T(8,128)(2,1)}) custom-call(bf16[192,2048]{1,0:T(8,128)(2,1)} %refs_0_.1, bf16[192,2048]{1,0:T(8,128)(2,1)} %refs_1_.1, ...), custom_call_target="tpu_custom_call" | custom-call | tf_op jit(solution)/shard_map/step/pallas_call | solution.py:609
  134.6 0.0 copy-start.1
  134.6 2.4 %copy.28 = bf16[1,2048,256]{2,1,0:T(8,128)(2,1)} copy(bf16[1,2048,256]{2,1,0:T(8,128)(2,1)} %bitcast.11) | data formatting | bytes 2097152
  137.0 0.0 copy-done.1
  137.0 0.0 copy-start
  137.0 1.0 copy.29
  138.0 0.6 copy-done
  138.6 0.0 copy-start.4
  138.6 0.0 copy-start.3
  138.6 1.0 copy.30
  139.6 0.0 copy-done.4
  139.6 0.6 copy.31
  140.2 0.0 copy-done.3
  140.2 0.6 copy.32
  140.8 0.2 copy-done.2
  141.0 0.6 copy.33
  (2 shorter events, 0.0 us)
Async XLA Ops:
  0.6 0.7 copy-start.7
  0.6 1.3 copy-start.5
  1.9 0.7 copy-start.6
  134.6 2.4 %copy-start.1 = (bf16[2048,256]{1,0:T(8,128)(2,1)S(1)}, bf16[2048,256]{1,0:T(8,128)(2,1)}, u32[]{:S(2)}) copy-start(bf16[2048,256]{1,0:T(8,128)(2,1)} %get-tuple-element.13) | copy-start | bytes 3145732
  137.0 1.6 %copy-start = (bf16[256,2048]{1,0:T(8,128)(2,1)S(1)}, bf16[256,2048]{1,0:T(8,128)(2,1)}, u32[]{:S(2)}) copy-start(bf16[256,2048]{1,0:T(8,128)(2,1)} %get-tuple-element.14) | copy-start | bytes 3145732
  138.6 1.0 copy-start.4
  138.6 1.6 %copy-start.3 = (bf16[192,128]{1,0:T(8,128)(2,1)S(1)}, bf16[192,128]{1,0:T(8,128)(2,1)}, u32[]{:S(2)}) copy-start(bf16[192,128]{1,0:T(8,128)(2,1)} %get-tuple-element.28) | copy-start | bytes 147460
  140.2 0.8 copy-start.2

commit v2 on v1

v2 whole, which is shorter than its diff:
```python
import functools
import math

import jax
import jax.numpy as jnp
from jax import lax
from jax.experimental import pallas as pl
from jax.experimental.pallas import tpu as pltpu
from jax.sharding import PartitionSpec as P

RATE_SCALE = 8.0
CLAMP_LIMIT = 7.0
SHARPNESS = 1.702
NORM_EPSILON = 1e-06
STATE_FLOOR = 0.001
GELU_CUBIC = 0.044715
GELU_SCALE = 0.7978845608028654

F32 = jnp.float32
BF16 = jnp.bfloat16
MESH = pl.DeviceIdType.MESH


def dot(a, b, ca=1, cb=0):
    return lax.dot_general(a, b, (((ca,), (cb,)), ((), ())), preferred_element_type=F32)


def gelu_parts(values):
    inside = GELU_SCALE * (values + GELU_CUBIC * values * values * values)
    tangent = jnp.tanh(inside)
    result = 0.5 * values * (1.0 + tangent)
    slope_value = 0.5 * (1.0 + tangent) + 0.5 * values * (1.0 - tangent * tangent) * GELU_SCALE * (
        1.0 + 3.0 * GELU_CUBIC * values * values
    )
    return (result, slope_value)


def less_one(x):
    series = jnp.ones_like(x)
    for n in range(8, 1, -1):
        series = 1.0 + x * (1.0 / n) * series
    return jnp.where(jnp.abs(x) < 0.35, x * series, jnp.exp(x) - 1.0)


def softplus_of_minus(x):
    return jnp.maximum(-x, 0.0) + jnp.log1p(jnp.exp(-jnp.abs(x)))


class Sizes:
    def __init__(self, tok, d, ns, ny, room, ffl, ch):
        self.tok, self.d, self.ns, self.ny, self.room = tok, d, ns, ny, room
        self.ffl, self.ch = ffl, ch
        self.nj = math.isqrt(ns)
        self.nz = ns // self.nj
        self.bl = self.nj * room
        self.sl = ns * room
        self.hs = self.sl // 2
        self.ht = tok // 2
        self.nk = 2 * ny
        self.c = d // self.nk
        self.w = self.c // 2
        self.via = 7
        self.nq = self.via + ny
        self.r = d // ns
        self.steps = [1 << i for i in range((tok - 1).bit_length())]


class Book:
    def __init__(self):
        self.n = 0

    def take(self, count):
        at, self.n = self.n, self.n + count
        return at


def layout(s):
    b, g = Book(), Book()
    arrivals = dict(
        s1=b.take(s.nq), s2=b.take(s.nq), y=b.take(3 * s.via), rs=b.take(16), sa=b.take(4),
        sb=b.take(4), tg=b.take(1), cm=b.take(1), ks=b.take(1), adj=b.take(1), pj=b.take(s.nz),
        pz=b.take(1),
    )
    groups = {name: g.take(1) for name in (
        "s1", "s2", "yu", "yd", "yr", "rs", "sa", "sb", "tg", "cm", "ks", "adj", "pj", "pz")}
    return arrivals, b.n, groups, g.n


def kernel(s, *refs):
    (mid_h, og_h, ids_h, rw_h, wg_hbm, wu_hbm, wd_hbm, outp_h, bgate_h, conv_h, prior_h, rgw_h,
     igw_h, dpar_h, djump_h, taps_h,
     gg_o, ug_o, dg_o, proj_o, ig_o, bgg_o,
     gg, ug, dg, proj_out, ig_out, bgg_out,
     mid, og, ids, rw, outp, bgate, conv, prior, rgw, igw, dpar, djump, taps,
     wgu, wd, inv_s, sel, gate, perm, s1, r1, s2, r2, xa, gu, ag, delta, act,
     p2, rt2, rb2, sp1, sm1, ft, fm, fo, rl, rr, s3, r3, s4, r4, tg,
     bd, gel, sslope, mixed, pst, ks, dec, adj, cms, cmr,
     cgr, pf, pr, ps2, pr2,
     ssem, rsem, lsem) = refs
    at, _, out, _ = layout(s)
    sp = lax.axis_index("sp")
    y = lax.axis_index("tp")
    z, j = sp // s.nj, sp % s.nj
    up, down = (y + 1) % s.ny, (y + s.ny - 1) % s.ny
    opp = (y + 2) % s.ny
    nxt, prv = (sp + 1) % s.ns, (sp + s.ns - 1) % s.ns

    def on_sp(i):
        return {"sp": i}

    def on_tp(i):
        return {"tp": i}

    def in_line(i):
        return {"sp": i * s.nj + j}

    def in_plane(i):
        return {"sp": z * s.nj + i}

    def send(src, dst, group, ri, dev):
        pltpu.make_async_remote_copy(
            src_ref=src, dst_ref=dst, send_sem=ssem.at[out[group]], recv_sem=rsem.at[ri],
            device_id=dev, device_id_type=MESH).start()

    def all_of(ref, group, ri):
        return pltpu.make_async_remote_copy(
            src_ref=ref, dst_ref=ref, send_sem=ssem.at[out[group]], recv_sem=rsem.at[ri],
            device_id=on_tp(up), device_id_type=MESH)

    def recv(ref, ri):
        all_of(ref, "s1", ri).wait_recv()

    def sent(ref, group):
        all_of(ref, group, 0).wait_send()

    def orders(n):
        half = n // 2
        out = [half]
        for d in range(half - 1, 0, -1):
            out += [d, n - d]
        return out if n > 2 else [1]

    def fetch(n, src, dst):
        cp = pltpu.make_async_copy(src, dst, lsem.at[n])
        cp.start()
        return cp

    barrier = pltpu.get_barrier_semaphore()
    partners = [in_line((z + d) % s.nz) for d in range(1, s.nz)]
    partners += [in_plane((j + d) % s.nj) for d in range(1, s.nj)]
    partners += [on_tp(up), on_tp(down), on_sp(nxt), on_sp(prv)]
    for dev in partners:
        pl.semaphore_signal(barrier, inc=1, device_id=dev, device_id_type=MESH)
    first = [fetch(0, ids_h, ids), fetch(1, rw_h, rw), fetch(2, mid_h, mid), fetch(3, og_h, og)]
    second = [fetch(n + 4, src, dst) for n, (src, dst) in enumerate((
        (bgate_h, bgate), (conv_h, conv), (prior_h, prior), (rgw_h, rgw), (igw_h, igw),
        (dpar_h, dpar), (djump_h, djump), (taps_h, taps), (outp_h, outp)))]
    loads = [
        fetch(13, wg_hbm, wgu.at[:, pl.ds(0, s.ffl)]),
        fetch(14, wu_hbm, wgu.at[:, pl.ds(s.ffl, s.ffl)]),
        fetch(15, wd_hbm, wd),
    ]
    first[0].wait()
    first[1].wait()

    ids0, ids1 = ids[0:1, :].astype(F32), ids[1:2, :].astype(F32)
    w0, w1 = rw[0:1, :], rw[1:2, :]
    names = lax.broadcasted_iota(jnp.int32, (s.ns, s.tok), 0).astype(F32)
    hit0, hit1 = names == ids0, names == ids1
    hits = jnp.where(hit0 | hit1, 1.0, 0.0)
    before = jnp.where(
        lax.broadcasted_iota(jnp.int32, (s.tok, s.tok), 0)
        < lax.broadcasted_iota(jnp.int32, (s.tok, s.tok), 1), 1.0, 0.0)
    counts = dot(hits.astype(BF16), before.astype(BF16))
    slot0 = ids0 * s.room + jnp.sum(jnp.where(hit0, counts, 0.0), axis=0, keepdims=True)
    slot1 = ids1 * s.room + jnp.sum(jnp.where(hit1, counts, 0.0), axis=0, keepdims=True)
    rows = lax.broadcasted_iota(jnp.int32, (s.sl, s.tok), 0).astype(F32)
    own0, own1 = rows == slot0, rows == slot1
    sel[...] = jnp.where(own0 | own1, 1.0, 0.0).astype(BF16)
    gate[...] = jnp.sum(jnp.where(own0, w0, 0.0) + jnp.where(own1, w1, 0.0), axis=1, keepdims=True)
    line = lax.broadcasted_iota(jnp.int32, (s.sl, 1), 0).astype(F32)
    outer = jnp.floor((line + 0.5) * (1.0 / s.bl))
    rest = line - outer * s.bl
    inner = jnp.floor((rest + 0.5) * (1.0 / s.room))
    source = inner * s.bl + outer * s.room + (rest - inner * s.room)
    perm[...] = jnp.where(
        lax.broadcasted_iota(jnp.int32, (s.sl, s.sl), 1).astype(F32) == source, 1.0, 0.0
    ).astype(BF16)

    first[2].wait()
    squares = jnp.zeros((s.tok, s.c), F32)
    for k in range(s.nk):
        part = mid[:, k * s.c:(k + 1) * s.c].astype(F32)
        squares = squares + part * part
    inv = lax.rsqrt(jnp.sum(squares, axis=1, keepdims=True) * (1.0 / s.d) + NORM_EPSILON)
    inv_s[...] = jnp.broadcast_to(inv, inv_s.shape)

    def quarter(c):
        return pl.ds(pl.multiple_of((y * 2 + c) * s.c, s.c), s.c)

    def source_of(i):
        return (y + i) % s.ny

    def blocks(x):
        return x.reshape(-1, s.bl, s.w).astype(BF16)

    def flat(ref):
        return ref.astype(F32).reshape(s.sl, s.w).astype(BF16)

    def half(i):
        return slice(i * s.w, (i + 1) * s.w)

    def toss(q, value):
        s1[q] = blocks(value)
        if q == 0:
            pl.semaphore_wait(barrier, len(partners))
        for d in orders(s.nz):
            zd = (z + d) % s.nz
            send(s1.at[q, zd], r1.at[q, z], "s1", at["s1"] + q, in_line(zd))
        r1[q, z] = s1[q, z]

    for pair in range(4):
        c, kind = pair // 2, pair % 2
        if kind == 0:
            piece = (mid[:, quarter(c)].astype(F32) * inv_s[:, 0:1]).astype(BF16)
            value = dot(sel[...], piece)
        else:
            if pair == 1:
                first[3].wait()
            value = dot(sel[...], og[:, quarter(c)]) * gate[...]
        for h in range(2):
            if 2 * pair + h < s.via:
                toss(2 * pair + h, value[:, half(h)])
            else:
                toss(s.via, value[:, half(h)])
    for i in range(1, s.ny):
        cols = pl.ds(pl.multiple_of((source_of(i) * 2 + 1) * s.c + s.w, s.w), s.w)
        toss(s.via + i, dot(sel[...], og[:, cols]) * gate[...])

    for cp in second:
        cp.wait()
    for side in range(2):
        for n, w in enumerate((rgw, igw)):
            zero = jnp.zeros((w.shape[2], w.shape[3]), F32)
            top = jnp.concatenate([w[side, 0].astype(F32), zero], axis=1)
            low = jnp.concatenate([zero, w[side, 1].astype(F32)], axis=1)
            bd[2 * side + n] = jnp.concatenate([top, low], axis=0).astype(BF16)
    gelu_value, gelu_slope = gelu_parts(bgate[...].astype(F32))
    gel[...] = gelu_value
    both_states = jnp.zeros((s.tok, s.ch), F32)
    mine = (slice(0, s.tok), slice(8, 8 + s.tok))
    front, back = pl.ds(0, 8), pl.ds(s.tok, 8)
    time = lax.broadcasted_iota(jnp.int32, (s.tok, s.ch), 0)
    for side in range(2):
        conv_b = conv[side]
        conv_f = conv_b.astype(F32)
        rate_gate = jax.nn.sigmoid(dot(conv_b, bd[2 * side]))
        input_gate = jax.nn.sigmoid(dot(conv_b, bd[2 * side + 1]))
        decay_rate = softplus_of_minus(dpar[side:side + 1, :])
        log_decay = -RATE_SCALE * rate_gate * decay_rate + djump[side]
        factors = jnp.exp(log_decay)
        squared = jnp.exp(2.0 * log_decay)
        norm_factor = jnp.sqrt(STATE_FLOOR - less_one(2.0 * log_decay))
        drive = input_gate * conv_f
        carried = factors * prior[side]
        both_states = both_states + (carried + norm_factor * drive)
        ks[side, 1, mine[side], :] = (carried - drive * squared / norm_factor) * (
            -RATE_SCALE * decay_rate) * rate_gate * (1.0 - rate_gate)
        ks[side, 2, mine[side], :] = norm_factor * conv_f * input_gate * (1.0 - input_gate)
        ks[side, 3, mine[side], :] = norm_factor * input_gate
        if side == 0:
            link = jnp.where(time < s.tok - 1, pltpu.roll(factors, s.tok - 1, 0), 1.0)
            dec[0:1, :] = factors[0:1, :]
        else:
            link = jnp.where(time > 0, pltpu.roll(factors, 1, 0), 1.0)
            dec[1:2, :] = factors[s.tok - 1:s.tok, :]
        for n, d in enumerate(s.steps):
            inside = time < s.tok - d if side == 0 else time >= d
            pst[side, n] = jnp.where(inside, link, 0.0)
            shift = s.tok - d if side == 0 else d
            link = jnp.where(inside, link * pltpu.roll(link, shift, 0), link)
        ks[side, 0, mine[side], :] = link
    sslope[...] = both_states * gelu_slope
    mixed[...] = (both_states * gelu_value).astype(BF16)
    send(ks.at[0, :, front], ks.at[0, :, back], "ks", at["ks"], on_sp(prv))
    send(ks.at[1, :, back], ks.at[1, :, front], "ks", at["ks"], on_sp(nxt))

    def turn(q):
        recv(r1.at[q, pl.ds(0, s.nz - 1)], at["s1"] + q)
        s2[q] = blocks(dot(perm[...], flat(r1[q])))
        for d in orders(s.nj):
            jd = (j + d) % s.nj
            send(s2.at[q, jd], r2.at[q, j], "s2", at["s2"] + q, in_plane(jd))
        r2[q, j] = s2[q, j]

    top, low = pl.ds(0, s.hs), pl.ds(s.hs, s.hs)

    def tile_of(q, y_of):
        pair, h = q // 2, q % 2
        return xa.at[pair % 2, y_of * 2 + pair // 2, :, half(h)]

    def rows_of(ref, part):
        return ref.at[part]

    def spread(q):
        recv(r2.at[q, pl.ds(0, s.nj - 1)], at["s2"] + q)
        if q >= s.via:
            xa[1, source_of(q - s.via) * 2 + 1, :, half(1)] = flat(r2[q])
            return
        pair, h = q // 2, q % 2
        xa[pair % 2, y * 2 + pair // 2, :, half(h)] = flat(r2[q])
        ref = tile_of(q, y)
        n = at["y"] + 3 * q
        send(ref, ref, "yu", n, on_tp(up))
        send(ref, ref, "yd", n + 1, on_tp(down))

    def relay(q):
        n = at["y"] + 3 * q
        ref = tile_of(q, down)
        recv(ref, n)
        send(ref.at[top], ref.at[top], "yr", n + 2, on_tp(up))
        ref = tile_of(q, up)
        recv(ref, n + 1)
        send(ref.at[low], ref.at[low], "yr", n + 2, on_tp(down))

    def arrive(q):
        recv(tile_of(q, opp), at["y"] + 3 * q + 2)

    def weights_of(k):
        return wgu[pl.ds(pl.multiple_of(k * s.c, s.c), s.c), :]

    def take(pair, places):
        c, kind = pair // 2, pair % 2
        for i, place in enumerate(places):
            k = place * 2 + c
            if kind == 0:
                value = dot(xa[0, k], weights_of(k))
                total = gu
            else:
                value = dot(xa[1, k], wd[:, pl.ds(pl.multiple_of(k * s.c, s.c), s.c)], 1, 1)
                total = ag
            if c == 0 and i == 0 and places[0] is y:
                total[...] = value
            else:
                total[...] += value

    def take_half(place, h):
        k = place * 2 + 1
        cols = pl.ds(pl.multiple_of(k * s.c + h * s.w, s.w), s.w)
        ag[...] += dot(xa[1, k, :, half(h)], wd[:, cols], 1, 1)

    turn(0)
    spread(0)
    turn(1)
    spread(1)
    turn(2)
    relay(0)
    spread(2)
    turn(3)
    relay(1)
    spread(3)
    turn(4)
    for cp in loads:
        cp.wait()
    relay(2)
    spread(4)
    turn(5)
    take(0, [y, up, down])
    relay(3)
    spread(5)
    turn(6)
    turn(7)
    spread(6)
    arrive(0)
    arrive(1)
    take(0, [opp])
    turn(8)
    relay(4)
    spread(7)
    turn(9)
    take(1, [y, up, down])
    relay(5)
    spread(8)
    turn(10)
    arrive(2)
    arrive(3)
    take(1, [opp])
    take(2, [y, up, down])
    spread(9)
    relay(6)
    take_half(source_of(0), 1)
    take_half(source_of(1), 1)
    arrive(4)
    arrive(5)
    take(2, [opp])
    for place in (y, up, down):
        take_half(place, 0)
    take_half(source_of(2), 1)
    spread(10)
    take_half(source_of(3), 1)
    arrive(6)
    take_half(opp, 0)

    gate_pre, up_pre = gu[:, :s.ffl], gu[:, s.ffl:]
    act_grad = ag[...]
    gate_clamped = jnp.minimum(gate_pre, CLAMP_LIMIT)
    up_clamped = jnp.clip(up_pre, -CLAMP_LIMIT, CLAMP_LIMIT)
    gate_sigmoid = jax.nn.sigmoid(SHARPNESS * gate_clamped)
    swish_value = gate_clamped * gate_sigmoid
    act[...] = ((up_clamped + 1.0) * swish_value).astype(BF16)
    delta[:, :s.ffl] = jnp.where(
        gate_pre < CLAMP_LIMIT,
        act_grad * (up_clamped + 1.0)
        * (gate_sigmoid + SHARPNESS * swish_value * (1.0 - gate_sigmoid)), 0.0).astype(BF16)
    delta[:, s.ffl:] = jnp.where(
        jnp.abs(up_pre) < CLAMP_LIMIT, act_grad * swish_value, 0.0).astype(BF16)

    def partial(owner, c):
        return dot(delta[...], weights_of(owner * 2 + c), 1, 1)

    def far_partial(c):
        p2[c] = partial(opp, c).astype(BF16)

    def near_partials(c):
        value = partial(up, c)
        sp1[c, s.hs:, :] = value[s.hs:].astype(BF16)
        ft[c] = value[:s.hs]
        value = partial(down, c)
        sm1[c, :s.hs, :] = value[:s.hs].astype(BF16)
        fm[c] = value[s.hs:]

    def send_far(i):
        c, h = i // 2, half(i % 2)
        n = at["rs"] + 4 * i
        send(p2.at[c, top, h], rt2.at[c, :, h], "rs", n, on_tp(up))
        send(p2.at[c, low, h], rb2.at[c, :, h], "rs", n + 1, on_tp(down))

    def send_near(i):
        c, h = i // 2, half(i % 2)
        n = at["rs"] + 4 * i
        send(sp1.at[c, low, h], rl.at[c, low, h], "rs", n + 2, on_tp(up))
        send(sm1.at[c, top, h], rr.at[c, top, h], "rs", n + 3, on_tp(down))

    def pass_on(i):
        c, h = i // 2, half(i % 2)
        n = at["rs"] + 4 * i
        recv(rt2.at[c, :, h], n)
        sp1[c, :s.hs, h] = (ft[c, :, h] + rt2[c, :, h].astype(F32)).astype(BF16)
        send(sp1.at[c, top, h], rl.at[c, top, h], "rs", n + 2, on_tp(up))
        recv(rb2.at[c, :, h], n + 1)
        sm1[c, s.hs:, h] = (fm[c, :, h] + rb2[c, :, h].astype(F32)).astype(BF16)
        send(sm1.at[c, low, h], rr.at[c, low, h], "rs", n + 3, on_tp(down))

    def own_partial(c):
        fo[c] = partial(y, c)

    def weight_grads(lo, hi):
        @pl.loop(lo, hi)
        def _(k):
            value = dot(xa[0, k], delta[...], 0, 0)
            where = pl.ds(pl.multiple_of(k * s.c, s.c), s.c)
            gg[where, :] = value[:, :s.ffl].astype(BF16)
            ug[where, :] = value[:, s.ffl:].astype(BF16)

    def down_grads(lo, hi):
        @pl.loop(lo, hi)
        def _(k):
            value = dot(act[...], xa[1, k], 0, 0)
            dg[:, pl.ds(pl.multiple_of(k * s.c, s.c), s.c)] = value.astype(BF16)

    stores = [
        pltpu.make_async_copy(src, dst, lsem.at[n]) for n, (src, dst) in enumerate((
            (gg, gg_o), (ug, ug_o), (dg, dg_o), (proj_out, proj_o), (ig_out, ig_o), (bgg_out, bgg_o)))]

    def put(n):
        stores[n].start()

    def give(i):
        c, h = i // 2, half(i % 2)
        n = at["rs"] + 4 * i
        recv(rl.at[c, :, h], n + 2)
        recv(rr.at[c, :, h], n + 3)
        s3[i] = blocks(fo[c, :, h] + rl[c, :, h].astype(F32) + rr[c, :, h].astype(F32))
        for d in orders(s.nj):
            jd = (j + d) % s.nj
            send(s3.at[i, jd], r3.at[i, j], "sa", at["sa"] + i, in_plane(jd))
        r3[i, j] = s3[i, j]

    def turn_back(i):
        recv(r3.at[i, pl.ds(0, s.nj - 1)], at["sa"] + i)
        s4[i] = blocks(dot(perm[...], flat(r3[i])))
        for d in orders(s.nz):
            zd = (z + d) % s.nz
            send(s4.at[i, zd], r4.at[i, z], "sb", at["sb"] + i, in_line(zd))
        r4[i, z] = s4[i, z]

    def tg_of(i, y_of):
        return tg.at[y_of * 2 + i // 2, :, half(i % 2)]

    def combine(i):
        recv(r4.at[i, pl.ds(0, s.nz - 1)], at["sb"] + i)
        tg[y * 2 + i // 2, :, half(i % 2)] = dot(sel[...], flat(r4[i]), 0, 0).astype(BF16)
        ref = tg_of(i, y)
        for to in (opp, up, down):
            send(ref, ref, "tg", at["tg"], on_tp(to))

    far_partial(0)
    send_far(0)
    near_partials(0)
    send_near(0)
    send_far(1)
    far_partial(1)
    own_partial(0)
    pass_on(0)
    send_near(1)
    send_far(2)
    near_partials(1)
    own_partial(1)
    weight_grads(0, s.nk // 4)
    pass_on(1)
    send_near(2)
    send_far(3)
    give(0)
    weight_grads(s.nk // 4, s.nk)
    put(0)
    put(1)
    pass_on(2)
    send_near(3)
    give(1)
    turn_back(0)
    down_grads(0, s.nk // 2)
    pass_on(3)
    give(2)
    turn_back(1)
    down_grads(s.nk // 2, s.nk)
    put(2)
    give(3)
    turn_back(2)
    combine(0)
    turn_back(3)
    combine(1)
    combine(2)
    combine(3)
    recv(tg.at[pl.ds(0, s.nk - 2)], at["tg"])

    inv_col = inv_s[:, 0:1]
    prods = jnp.zeros((s.tok, s.c), F32)
    for k in range(s.nk):
        part = mid[:, k * s.c:(k + 1) * s.c].astype(F32) * inv_col
        prods = prods + tg[k].astype(F32) * part
    inner_mean = jnp.sum(prods, axis=1, keepdims=True) * (1.0 / s.d)
    branch_grad = jnp.zeros((s.tok, s.ch), F32)
    per = s.nk // s.nz
    turns = orders(s.nz) + [0]
    step = max(1, s.nz // 2)
    for lot in (turns[:step], turns[step:]):
        for d in lot:
            zd = (z + d) % s.nz
            for i in range(per):
                k = zd * per + i
                cols = pl.ds(pl.multiple_of(k * s.c, s.c), s.c)
                part = mid[:, cols].astype(F32) * inv_col
                value = (og[:, cols].astype(F32)
                         + inv_col * (tg[k].astype(F32) - part * inner_mean)).astype(BF16)
                branch_grad = branch_grad + dot(value, outp[:, cols], 1, 1)
                value = dot(value, mixed[...], 0, 0).astype(BF16)
                if per == 1:
                    pf[zd] = value.reshape(s.nj, s.r, s.ch)
                else:
                    pf[zd, i * s.c // s.r, pl.ds(i * s.c % s.r, s.c), :] = value
        for d in lot:
            zd = (z + d) % s.nz
            for e in orders(s.nj):
                jd = (j + e) % s.nj
                send(pf.at[zd, jd], pr.at[j, zd], "pj", at["pj"] + zd, in_plane(jd))
            pr[j, zd] = pf[zd, j]
    bgg_out[...] = (branch_grad * sslope[...]).astype(BF16)
    put(5)
    state_grad = branch_grad * gel[...]

    for side in range(2):
        chain = state_grad
        for n, d in enumerate(s.steps):
            shift = s.tok - d if side == 0 else d
            chain = chain + pst[side, n] * pltpu.roll(chain, shift, 0)
        adj[side, mine[side], :] = chain
        edge = slice(0, 1) if side == 0 else slice(s.tok - 1, s.tok)
        edge_of = mine[side].start + edge.start
        cms[side, 0:1, :] = dec[side:side + 1, :] * ks[side, 0, edge_of:edge_of + 1, :]
        cms[side, 1:2, :] = dec[side:side + 1, :] * chain[edge]
    send(adj.at[0, front], adj.at[0, back], "adj", at["adj"], on_sp(prv))
    send(adj.at[1, back], adj.at[1, front], "adj", at["adj"], on_sp(nxt))
    for d in orders(s.nz) + [0]:
        for e in range(s.nj):
            if d or e:
                to = ((z + d) % s.nz) * s.nj + (j + e) % s.nj
                send(cms.at[jnp.where(to < sp, 0, 1)], cmr.at[sp], "cm", at["cm"], on_sp(to))

    for d in orders(s.nz) + [0]:
        zd = (z + d) % s.nz
        recv(pr.at[pl.ds(0, s.nj - 1), zd], at["pj"] + zd)
        total = pr[0, zd].astype(F32)
        for i in range(1, s.nj):
            total = total + pr[i, zd].astype(F32)
        ps2[zd] = total.astype(BF16)
        if d:
            send(ps2.at[zd], pr2.at[z], "pz", at["pz"], in_line(zd))
        else:
            pr2[z] = ps2[zd]

    recv(cmr.at[pl.ds(0, s.ns - 1)], at["cm"])
    recv(ks.at[:, :, front], at["ks"])
    recv(adj.at[:, front], at["adj"])

    nil = jnp.zeros((1, s.ch), F32)
    later, later_next = nil, nil
    for i in range(s.ns - 1, 0, -1):
        a = jnp.where(i > sp, cmr[i, 0:1, :], 1.0)
        b = jnp.where(i > sp, cmr[i, 1:2, :], 0.0)
        later = a * later + b
        later_next = jnp.where(i > sp + 1, later, later_next)
    earlier, earlier_next = nil, nil
    for i in range(s.ns - 1):
        a = jnp.where(i < sp, cmr[i, 0:1, :], 1.0)
        b = jnp.where(i < sp, cmr[i, 1:2, :], 0.0)
        earlier = a * earlier + b
        earlier_next = jnp.where(i < sp - 1, earlier, earlier_next)
    place = lax.broadcasted_iota(jnp.int32, (s.tok + 8, s.ch), 0)
    for side in range(2):
        if side == 0:
            own, inflow = place < s.tok, (later, later_next)
            live = own | (sp < s.ns - 1)
        else:
            own, inflow = place >= 8, (earlier, earlier_next)
            live = own | (sp > 0)
        adjoint = adj[side] + ks[side, 0] * jnp.where(own, inflow[0], inflow[1])
        rate_pre = (adjoint * ks[side, 1]).astype(BF16)
        input_pre = (adjoint * ks[side, 2]).astype(BF16)
        value = (adjoint * ks[side, 3] + dot(rate_pre, bd[2 * side], 1, 1)
                 + dot(input_pre, bd[2 * side + 1], 1, 1))
        cgr[side] = jnp.where(live, value, 0.0)
    reach = taps.shape[1] - 1
    tap = taps[...].astype(F32)
    result = jnp.zeros((s.tok, s.ch), F32)
    for t in range(reach + 1):
        off = reach - t
        result = (result + tap[0, t:t + 1, :] * cgr[0, off:off + s.tok, :]
                  + tap[1, t:t + 1, :] * cgr[1, 8 - off:8 - off + s.tok, :])
    ig_out[...] = result.astype(BF16)
    put(4)

    recv(pr2.at[pl.ds(0, s.nz - 1)], at["pz"])
    total = pr2[0].astype(F32)
    for i in range(1, s.nz):
        total = total + pr2[i].astype(F32)
    proj_out[...] = total
    put(3)

    for cp in stores:
        cp.wait()
    line, plane = pl.ds(0, s.nz - 1), pl.ds(0, s.nj - 1)
    sent(s1.at[:, line], "s1")
    sent(s2.at[:, plane], "s2")
    for group in ("yu", "yd", "yr"):
        sent(xa.at[0, pl.ds(0, s.via), :, half(0)], group)
    sent(xa.at[0, pl.ds(0, 6)], "rs")
    sent(s3.at[:, plane], "sa")
    sent(s4.at[:, line], "sb")
    sent(tg.at[pl.ds(0, 6)], "tg")
    sent(cmr.at[pl.ds(0, s.ns - 1)], "cm")
    sent(ks.at[:, :, front], "ks")
    sent(adj.at[:, front], "adj")
    sent(pf.at[:, plane], "pj")
    sent(ps2.at[line], "pz")


def on_device(mid, out_grad, expert_ids, route_weights, gate_proj, up_proj, down_proj, out_proj,
              branch_gate, conv_out, prior_state, rate_gate_w, input_gate_w, decay_param,
              decay_jump, conv_taps):
    tok, d = mid.shape
    ns, ny = lax.axis_size("sp"), lax.axis_size("tp")
    room = 3 * expert_ids.shape[1] * tok // (2 * ns)
    ffl, ch = gate_proj.shape[2], out_proj.shape[0]
    s = Sizes(tok, d, ns, ny, room, ffl, ch)
    _, count, _, groups = layout(s)
    vm, hbm = pl.BlockSpec(memory_space=pltpu.VMEM), pl.BlockSpec(memory_space=pl.ANY)
    nst = len(s.steps)

    def b(*shape):
        return pltpu.VMEM(shape, BF16)

    def f(*shape):
        return pltpu.VMEM(shape, F32)

    def like(x):
        return pltpu.VMEM(x.shape, x.dtype)

    inputs = (mid, out_grad, expert_ids.T, route_weights.T, gate_proj[0], up_proj[0], down_proj[0],
              out_proj, branch_gate, conv_out, prior_state, rate_gate_w, input_gate_w, decay_param,
              decay_jump, conv_taps)
    scratch = [like(x) for x in inputs[:4] + inputs[7:]] + [
        b(d, 2 * ffl), b(ffl, d), f(tok, 128), b(s.sl, tok), f(s.sl, 1), b(s.sl, s.sl),
        b(s.nq, s.nz, s.bl, s.w), b(s.nq, s.nz, s.bl, s.w), b(s.nq, s.nj, s.bl, s.w), b(s.nq, s.nj, s.bl, s.w),
        b(2, s.nk, s.sl, s.c), f(s.sl, 2 * ffl), f(s.sl, ffl), b(s.sl, 2 * ffl), b(s.sl, ffl),
        b(2, s.sl, s.c), b(2, s.hs, s.c), b(2, s.hs, s.c), b(2, s.sl, s.c), b(2, s.sl, s.c),
        f(2, s.hs, s.c), f(2, s.hs, s.c), f(2, s.sl, s.c), b(2, s.sl, s.c), b(2, s.sl, s.c),
        b(4, s.nj, s.bl, s.w), b(4, s.nj, s.bl, s.w), b(4, s.nz, s.bl, s.w), b(4, s.nz, s.bl, s.w),
        b(s.nk, tok, s.c),
        b(4, ch, ch), f(tok, ch), f(tok, ch), b(tok, ch), f(2, nst, tok, ch), f(2, 4, tok + 8, ch),
        f(2, ch), f(2, tok + 8, ch), f(2, 2, ch), f(ns, 2, ch),
        f(2, tok + 8, ch), b(s.nz, s.nj, s.r, ch), b(s.nj, s.nz, s.r, ch), b(s.nz, s.r, ch), b(s.nz, s.r, ch),
        pltpu.SemaphoreType.DMA((groups,)), pltpu.SemaphoreType.DMA((count,)),
        pltpu.SemaphoreType.DMA((16,)),
    ]
    shapes = (((d, ffl), BF16), ((d, ffl), BF16), ((ffl, d), BF16), ((s.r, ch), F32),
              ((tok, ch), BF16), ((tok, ch), BF16))
    scratch = [pltpu.VMEM(*x) for x in shapes] + scratch
    outs = pl.pallas_call(
        functools.partial(kernel, s),
        out_shape=tuple(pltpu.VMEM(*x) for x in shapes),
        in_specs=[hbm] * len(inputs),
        out_specs=(hbm,) * 6,
        scratch_shapes=scratch,
        compiler_params=pltpu.CompilerParams(
            collective_id=0, has_side_effects=True, vmem_limit_bytes=56 * 1024 * 1024),
        name="step",
    )(*inputs)
    outs = pl.pallas_call(
        write_out,
        out_shape=tuple(jax.ShapeDtypeStruct(*x) for x in shapes),
        in_specs=[hbm] * 6,
        out_specs=(hbm,) * 6,
        scratch_shapes=[pltpu.SemaphoreType.DMA((6,))],
        compiler_params=pltpu.CompilerParams(vmem_limit_bytes=1024 * 1024),
        name="write_out",
    )(*(pltpu.with_memory_space_constraint(x, pltpu.VMEM) for x in outs))
    gg, ug, dg, proj, ig, bgg = outs
    return gg[None], ug[None], dg[None], proj, ig, bgg


def write_out(*refs):
    copies = [pltpu.make_async_copy(refs[i], refs[6 + i], refs[12].at[i]) for i in range(6)]
    for cp in copies:
        cp.start()
    for cp in copies:
        cp.wait()


def solution(mesh):
    in_specs = (
        P("sp", None), P("sp", None), P("sp", None), P("sp", None),
        P("sp", None, "tp"), P("sp", None, "tp"), P("sp", "tp", None), P("tp", None),
        P("sp", "tp"), P(None, "sp", "tp"), P(None, "sp", "tp"), P(None, "tp", None, None),
        P(None, "tp", None, None), P(None, "tp"), P(None, "sp", "tp"), P(None, None, "tp"),
    )
    out_specs = (
        P("sp", None, "tp"), P("sp", None, "tp"), P("sp", "tp", None),
        P("sp", "tp"), P("sp", "tp"), P("sp", "tp"),
    )
    return jax.shard_map(
        on_device, mesh=mesh, in_specs=in_specs, out_specs=out_specs, check_vma=False
    )
```

time: 143 us -> 112 us (0.78)
  Pallas kernels: 131 us -> 111 us
  local copies, waits for them, and re-layouts: 8.32 us -> 0 us
    pallas_call x1 -> x2, Pallas kernels: 131 us -> 111 us  [the longest x1 109 us: on_device(): pl.pallas_call(functools.partial(kernel, s), out_shape=tuple((pltpu.VMEM(...]
    unnamed x22 -> x0, local copies, waits for them, and re-layouts: 8.32 us -> none
where the time goes in v2:
time: 112 us
  Pallas kernels  111 us (99%)
    pallas_call x1, Pallas kernels, on_device(): pl.pallas_call(functools.partial(kernel, s), out_shape=tuple((pltpu.VMEM(...  109 us

profile of v2, /device:TPU:1, one launch (start us, length us, event | category | flops | bytes accessed | tf_op | source)
XLA Modules:
  0.0 111.8 jit_solution(7474652799760071755)
XLA Ops:
  0.6 109.3 %step.1 = (bf16[2048,256]{1,0:T(8,128)(2,1)S(1)}, bf16[2048,256]{1,0:T(8,128)(2,1)S(1)}, bf16[256,2048]{1,0:T(8,128)(2,1)S(1)}, f32[32,128]{1,0:T(8,128)S(1)}, b...) custom-call(bf16[192,2048]{1,0:T(8,128)(2,1)} %refs_0_.1, bf16[192,2048]{1,0:T(8,128)(2,1)} %refs_1_.1, ...), custom_call_target="tpu_custom_call" | custom-call | tf_op jit(solution)/shard_map/step/pallas_call | solution.py:718
  109.9 1.7 %write_out.1 = (bf16[2048,256]{1,0:T(8,128)(2,1)}, bf16[2048,256]{1,0:T(8,128)(2,1)}, bf16[256,2048]{1,0:T(8,128)(2,1)}, f32[32,128]{1,0:T(8,128)}, bf16[192,128]{1,0:T(8,128)(2,1)}, /*index=5*/bf16[192,128]{1,0:T(8,128)(2,1)}) custom-call(bf16[2048,256]{1,0:T(8,128)(2,1)S(1)} %get-tuple-element.18.refs_0_, bf16[2048,256]{1,0:T(8,128)(2,1)S(1)} %get-tuple-element.19.refs_1_, ...), custom_call_target="tpu_custom_call" | custom-call | tf_op jit(solution)/shard_map/write_out/pallas_call | solution.py:728

commit v3 on v2

--- a/solution.py
+++ b/solution.py
@@ -60,7 +60,9 @@
         self.c = d // self.nk
         self.w = self.c // 2
         self.via = 7
-        self.nq = self.via + ny
+        self.nq = self.via + ny + 1
+        self.early = 3
+        self.across = self.nj // 2
         self.r = d // ns
         self.steps = [1 << i for i in range((tok - 1).bit_length())]
 
@@ -77,12 +79,12 @@
 def layout(s):
     b, g = Book(), Book()
     arrivals = dict(
-        s1=b.take(s.nq), s2=b.take(s.nq), y=b.take(3 * s.via), rs=b.take(16), sa=b.take(4),
-        sb=b.take(4), tg=b.take(1), cm=b.take(1), ks=b.take(1), adj=b.take(1), pj=b.take(s.nz),
-        pz=b.take(1),
+        s1=b.take(s.nq), s2=b.take(s.nq), s0=b.take(s.early * (s.nj // 2)), y=b.take(3 * s.via), rs=b.take(16), sa=b.take(6),
+        sb=b.take(6), tf=b.take(1), tg=b.take(4), cm=b.take(1), ks=b.take(1), adj=b.take(1), pj=b.take(s.nz),
+        pz=b.take(1), qz=b.take(1), qp=b.take(1),
     )
     groups = {name: g.take(1) for name in (
-        "s1", "s2", "yu", "yd", "yr", "rs", "sa", "sb", "tg", "cm", "ks", "adj", "pj", "pz")}
+        "s1", "s2", "yu", "yd", "yr", "rs", "sa", "sb", "tf", "tg", "cm", "ks", "adj", "pj", "pz", "qz", "qp")}
     return arrivals, b.n, groups, g.n
 
 
@@ -93,9 +95,9 @@
      gg, ug, dg, proj_out, ig_out, bgg_out,
      mid, og, ids, rw, outp, bgate, conv, prior, rgw, igw, dpar, djump, taps,
      wgu, wd, inv_s, sel, gate, perm, s1, r1, s2, r2, xa, gu, ag, delta, act,
-     p2, rt2, rb2, sp1, sm1, ft, fm, fo, rl, rr, s3, r3, s4, r4, tg,
+     p2, rt2, rb2, sp1, sm1, ft, fm, fo, rl, rr, s3, r3, s4, r4, tfs, tfr, tg,
      bd, gel, sslope, mixed, pst, ks, dec, adj, cms, cmr,
-     cgr, pf, pr, ps2, pr2,
+     cgr, pf, pr, ps2, pr2, qr, qs, qp,
      ssem, rsem, lsem) = refs
     at, _, out, _ = layout(s)
     sp = lax.axis_index("sp")
@@ -105,34 +107,6 @@
     opp = (y + 2) % s.ny
     nxt, prv = (sp + 1) % s.ns, (sp + s.ns - 1) % s.ns
 
-    def on_sp(i):
-        return {"sp": i}
-
-    def on_tp(i):
-        return {"tp": i}
-
-    def in_line(i):
-        return {"sp": i * s.nj + j}
-
-    def in_plane(i):
-        return {"sp": z * s.nj + i}
-
-    def send(src, dst, group, ri, dev):
-        pltpu.make_async_remote_copy(
-            src_ref=src, dst_ref=dst, send_sem=ssem.at[out[group]], recv_sem=rsem.at[ri],
-            device_id=dev, device_id_type=MESH).start()
-
-    def all_of(ref, group, ri):
-        return pltpu.make_async_remote_copy(
-            src_ref=ref, dst_ref=ref, send_sem=ssem.at[out[group]], recv_sem=rsem.at[ri],
-            device_id=on_tp(up), device_id_type=MESH)
-
-    def recv(ref, ri):
-        all_of(ref, "s1", ri).wait_recv()
-
-    def sent(ref, group):
-        all_of(ref, group, 0).wait_send()
-
     def orders(n):
         half = n // 2
         out = [half]
@@ -140,13 +114,41 @@
             out += [d, n - d]
         return out if n > 2 else [1]
 
+    def on_sp(i):
+        return {"sp": i}
+
+    def on_tp(i):
+        return {"tp": i}
+
+    def in_line(i):
+        return {"sp": i * s.nj + j}
+
+    def in_plane(i):
+        return {"sp": z * s.nj + i}
+
+    def send(src, dst, group, ri, dev):
+        pltpu.make_async_remote_copy(
+            src_ref=src, dst_ref=dst, send_sem=ssem.at[out[group]], recv_sem=rsem.at[ri],
+            device_id=dev, device_id_type=MESH).start()
+
+    def all_of(ref, group, ri):
+        return pltpu.make_async_remote_copy(
+            src_ref=ref, dst_ref=ref, send_sem=ssem.at[out[group]], recv_sem=rsem.at[ri],
+            device_id=on_tp(up), device_id_type=MESH)
+
+    def recv(ref, ri):
+        all_of(ref, "s1", ri).wait_recv()
+
+    def sent(ref, group):
+        all_of(ref, group, 0).wait_send()
+
     def fetch(n, src, dst):
         cp = pltpu.make_async_copy(src, dst, lsem.at[n])
         cp.start()
         return cp
 
     barrier = pltpu.get_barrier_semaphore()
-    partners = [in_line((z + d) % s.nz) for d in range(1, s.nz)]
+    partners = [in_line((z + d) % s.nz) for d in orders(s.nz)]
     partners += [in_plane((j + d) % s.nj) for d in range(1, s.nj)]
     partners += [on_tp(up), on_tp(down), on_sp(nxt), on_sp(prv)]
     for dev in partners:
@@ -201,6 +203,9 @@
     def source_of(i):
         return (y + i) % s.ny
 
+    def straight(i):
+        return (source_of(i), 1) if i < s.ny else (opp, 0)
+
     def blocks(x):
         return x.reshape(-1, s.bl, s.w).astype(BF16)
 
@@ -233,8 +238,9 @@
                 toss(2 * pair + h, value[:, half(h)])
             else:
                 toss(s.via, value[:, half(h)])
-    for i in range(1, s.ny):
-        cols = pl.ds(pl.multiple_of((source_of(i) * 2 + 1) * s.c + s.w, s.w), s.w)
+    for i in range(1, s.ny + 1):
+        owner, h = straight(i)
+        cols = pl.ds(pl.multiple_of((owner * 2 + 1) * s.c + h * s.w, s.w), s.w)
         toss(s.via + i, dot(sel[...], og[:, cols]) * gate[...])
 
     for cp in second:
@@ -288,10 +294,25 @@
     def turn(q):
         recv(r1.at[q, pl.ds(0, s.nz - 1)], at["s1"] + q)
         s2[q] = blocks(dot(perm[...], flat(r1[q])))
-        for d in orders(s.nj):
-            jd = (j + d) % s.nj
-            send(s2.at[q, jd], r2.at[q, j], "s2", at["s2"] + q, in_plane(jd))
+        for d in [1] + [i for i in orders(s.nj) if i != 1]:
+            jd = j ^ d
+            number = at["s0"] + q * (s.nj // 2) + j // 2 if q < s.early else at["s2"] + q
+            send(s2.at[q, jd], r2.at[q, j], "s2", number, in_plane(jd))
         r2[q, j] = s2[q, j]
+
+    def spread_early(q, lo, hi):
+        rows = 2 * s.bl
+        pair, h = q // 2, q % 2
+        for d in range(lo, hi):
+            x = (j // 2) ^ d
+            two = r2.at[q, pl.ds(2 * x, 2)]
+            recv(r2.at[q, j ^ 1] if d == 0 else two, at["s0"] + q * (s.nj // 2) + x)
+            part = pl.ds(pl.multiple_of(x * rows, rows), rows)
+            xa[pair % 2, y * 2 + pair // 2, part, half(h)] = (
+                two[...].astype(F32).reshape(rows, s.w).astype(BF16))
+            ref = tile_of(q, y).at[part]
+            send(ref, ref, "yu", at["y"] + 3 * q, on_tp(up))
+            send(ref, ref, "yd", at["y"] + 3 * q + 1, on_tp(down))
 
     top, low = pl.ds(0, s.hs), pl.ds(s.hs, s.hs)
 
@@ -305,7 +326,8 @@
     def spread(q):
         recv(r2.at[q, pl.ds(0, s.nj - 1)], at["s2"] + q)
         if q >= s.via:
-            xa[1, source_of(q - s.via) * 2 + 1, :, half(1)] = flat(r2[q])
+            owner, h = straight(q - s.via)
+            xa[1, owner * 2 + 1, :, half(h)] = flat(r2[q])
             return
         pair, h = q // 2, q % 2
         xa[pair % 2, y * 2 + pair // 2, :, half(h)] = flat(r2[q])
@@ -318,10 +340,12 @@
         n = at["y"] + 3 * q
         ref = tile_of(q, down)
         recv(ref, n)
-        send(ref.at[top], ref.at[top], "yr", n + 2, on_tp(up))
+        if q < s.via - 1:
+            send(ref.at[top], ref.at[top], "yr", n + 2, on_tp(up))
         ref = tile_of(q, up)
         recv(ref, n + 1)
-        send(ref.at[low], ref.at[low], "yr", n + 2, on_tp(down))
+        if q < s.via - 1:
+            send(ref.at[low], ref.at[low], "yr", n + 2, on_tp(down))
 
     def arrive(q):
         recv(tile_of(q, opp), at["y"] + 3 * q + 2)
@@ -349,57 +373,61 @@
         cols = pl.ds(pl.multiple_of(k * s.c + h * s.w, s.w), s.w)
         ag[...] += dot(xa[1, k, :, half(h)], wd[:, cols], 1, 1)
 
+    chips = s.nj // 2
     turn(0)
-    spread(0)
+    spread_early(0, 0, 1)
     turn(1)
-    spread(1)
+    spread_early(0, 1, chips)
+    spread_early(1, 0, 1)
     turn(2)
+    spread_early(1, 1, chips)
+    spread_early(2, 0, 1)
+    turn(3)
     relay(0)
-    spread(2)
-    turn(3)
+    spread_early(2, 1, chips)
+    turn(4)
+    spread(3)
     relay(1)
-    spread(3)
-    turn(4)
+    turn(5)
+    spread(4)
+    turn(6)
     for cp in loads:
         cp.wait()
     relay(2)
-    spread(4)
-    turn(5)
-    take(0, [y, up, down])
-    relay(3)
     spread(5)
-    turn(6)
     turn(7)
     spread(6)
+    relay(3)
+    turn(8)
+    take(0, [y, up, down])
+    turn(9)
+    relay(4)
+    spread(7)
     arrive(0)
     arrive(1)
     take(0, [opp])
-    turn(8)
-    relay(4)
-    spread(7)
-    turn(9)
+    turn(10)
+    spread(8)
+    relay(5)
+    turn(11)
     take(1, [y, up, down])
-    relay(5)
-    spread(8)
-    turn(10)
+    spread(9)
+    take(2, [y, up, down])
+    for i in range(3):
+        take_half(source_of(i), 1)
+    spread(10)
+    take_half(source_of(3), 1)
+    relay(6)
+    for place in (y, up, down):
+        take_half(place, 0)
+    spread(11)
+    take_half(opp, 0)
     arrive(2)
     arrive(3)
     take(1, [opp])
-    take(2, [y, up, down])
-    spread(9)
-    relay(6)
-    take_half(source_of(0), 1)
-    take_half(source_of(1), 1)
     arrive(4)
     arrive(5)
     take(2, [opp])
-    for place in (y, up, down):
-        take_half(place, 0)
-    take_half(source_of(2), 1)
-    spread(10)
-    take_half(source_of(3), 1)
-    arrive(6)
-    take_half(opp, 0)
 
     gate_pre, up_pre = gu[:, :s.ffl], gu[:, s.ffl:]
     act_grad = ag[...]
@@ -429,6 +457,21 @@
         sm1[c, :s.hs, :] = value[:s.hs].astype(BF16)
         fm[c] = value[s.hs:]
 
+    def near_full(c):
+        sp1[c] = partial(up, c).astype(BF16)
+        sm1[c] = partial(down, c).astype(BF16)
+
+    def send_full(i):
+        c, h = i // 2, half(i % 2)
+        n = at["rs"] + 4 * i
+        send(sp1.at[c, :, h], rl.at[c, :, h], "rs", n + 2, on_tp(up))
+        send(sm1.at[c, :, h], rr.at[c, :, h], "rs", n + 3, on_tp(down))
+
+    def far_direct(c):
+        value = partial(opp, c)
+        for h in range(2):
+            into_plane(4 + h, value[:, half(h)])
+
     def send_far(i):
         c, h = i // 2, half(i % 2)
         n = at["rs"] + 4 * i
@@ -480,7 +523,10 @@
         n = at["rs"] + 4 * i
         recv(rl.at[c, :, h], n + 2)
         recv(rr.at[c, :, h], n + 3)
-        s3[i] = blocks(fo[c, :, h] + rl[c, :, h].astype(F32) + rr[c, :, h].astype(F32))
+        into_plane(i, fo[c, :, h] + rl[c, :, h].astype(F32) + rr[c, :, h].astype(F32))
+
+    def into_plane(i, value):
+        s3[i] = blocks(value)
         for d in orders(s.nj):
             jd = (j + d) % s.nj
             send(s3.at[i, jd], r3.at[i, j], "sa", at["sa"] + i, in_plane(jd))
@@ -497,61 +543,77 @@
     def tg_of(i, y_of):
         return tg.at[y_of * 2 + i // 2, :, half(i % 2)]
 
+    def token_sums(i):
+        recv(r4.at[i, pl.ds(0, s.nz - 1)], at["sb"] + i)
+        return dot(sel[...], flat(r4[i]), 0, 0)
+
+    def combine_far(h):
+        tfs[h] = token_sums(4 + h).astype(BF16)
+        send(tfs.at[h], tfr.at[h], "tf", at["tf"], on_tp(opp))
+
     def combine(i):
-        recv(r4.at[i, pl.ds(0, s.nz - 1)], at["sb"] + i)
-        tg[y * 2 + i // 2, :, half(i % 2)] = dot(sel[...], flat(r4[i]), 0, 0).astype(BF16)
+        value = token_sums(i)
+        if i >= 2:
+            if i == 2:
+                recv(tfr, at["tf"])
+            value = value + tfr[i - 2].astype(F32)
+        tg[y * 2 + i // 2, :, half(i % 2)] = value.astype(BF16)
         ref = tg_of(i, y)
         for to in (opp, up, down):
-            send(ref, ref, "tg", at["tg"], on_tp(to))
+            send(ref, ref, "tg", at["tg"] + i, on_tp(to))
 
     far_partial(0)
     send_far(0)
     near_partials(0)
     send_near(0)
     send_far(1)
-    far_partial(1)
+    far_direct(1)
     own_partial(0)
+    near_full(1)
     pass_on(0)
     send_near(1)
-    send_far(2)
-    near_partials(1)
     own_partial(1)
     weight_grads(0, s.nk // 4)
     pass_on(1)
-    send_near(2)
-    send_far(3)
+    send_full(2)
+    send_full(3)
+    turn_back(4)
+    turn_back(5)
+    weight_grads(s.nk // 4, s.nk // 2)
     give(0)
-    weight_grads(s.nk // 4, s.nk)
+    weight_grads(s.nk // 2, s.nk)
     put(0)
     put(1)
-    pass_on(2)
-    send_near(3)
     give(1)
     turn_back(0)
     down_grads(0, s.nk // 2)
-    pass_on(3)
     give(2)
+    combine_far(0)
     turn_back(1)
-    down_grads(s.nk // 2, s.nk)
-    put(2)
+    combine_far(1)
     give(3)
     turn_back(2)
     combine(0)
+    down_grads(s.nk // 2, s.nk)
+    put(2)
     turn_back(3)
     combine(1)
     combine(2)
     combine(3)
-    recv(tg.at[pl.ds(0, s.nk - 2)], at["tg"])
-
     inv_col = inv_s[:, 0:1]
-    prods = jnp.zeros((s.tok, s.c), F32)
-    for k in range(s.nk):
-        part = mid[:, k * s.c:(k + 1) * s.c].astype(F32) * inv_col
-        prods = prods + tg[k].astype(F32) * part
+    prods = jnp.zeros((s.tok, s.w), F32)
+    for i in range(4):
+        recv(tg.at[pl.ds(0, s.ny - 1), :, half(0)], at["tg"] + i)
+        for owner in range(s.ny):
+            k, h = owner * 2 + i // 2, i % 2
+            part = mid[:, k * s.c + h * s.w:k * s.c + (h + 1) * s.w].astype(F32) * inv_col
+            prods = prods + tg[k, :, half(h)].astype(F32) * part
     inner_mean = jnp.sum(prods, axis=1, keepdims=True) * (1.0 / s.d)
     branch_grad = jnp.zeros((s.tok, s.ch), F32)
     per = s.nk // s.nz
     turns = orders(s.nz) + [0]
+    over = (j + s.across) % s.nj
+    beside = [e for e in orders(s.nj) if e != s.across]
     step = max(1, s.nz // 2)
     for lot in (turns[:step], turns[step:]):
         for d in lot:
@@ -570,7 +632,11 @@
                     pf[zd, i * s.c // s.r, pl.ds(i * s.c % s.r, s.c), :] = value
         for d in lot:
             zd = (z + d) % s.nz
-            for e in orders(s.nj):
+            if d:
+                send(pf.at[zd, over], qr.at[z], "qz", at["qz"], in_line(zd))
+            else:
+                qr[z] = pf[z, over]
+            for e in beside:
                 jd = (j + e) % s.nj
                 send(pf.at[zd, jd], pr.at[j, zd], "pj", at["pj"] + zd, in_plane(jd))
             pr[j, zd] = pf[zd, j]
@@ -598,15 +664,23 @@
 
     for d in orders(s.nz) + [0]:
         zd = (z + d) % s.nz
-        recv(pr.at[pl.ds(0, s.nj - 1), zd], at["pj"] + zd)
-        total = pr[0, zd].astype(F32)
-        for i in range(1, s.nj):
-            total = total + pr[i, zd].astype(F32)
+        if beside:
+            recv(pr.at[pl.ds(0, len(beside)), zd], at["pj"] + zd)
+        total = pr[j, zd].astype(F32)
+        for e in beside:
+            total = total + pr[(j + e) % s.nj, zd].astype(F32)
         ps2[zd] = total.astype(BF16)
         if d:
             send(ps2.at[zd], pr2.at[z], "pz", at["pz"], in_line(zd))
         else:
             pr2[z] = ps2[zd]
+
+    recv(qr.at[pl.ds(0, s.nz - 1)], at["qz"])
+    total = qr[0].astype(F32)
+    for i in range(1, s.nz):
+        total = total + qr[i].astype(F32)
+    qs[...] = total.astype(BF16)
+    send(qs, qp, "qp", at["qp"], in_plane(over))
 
     recv(cmr.at[pl.ds(0, s.ns - 1)], at["cm"])
     recv(ks.at[:, :, front], at["ks"])
@@ -653,6 +727,8 @@
     total = pr2[0].astype(F32)
     for i in range(1, s.nz):
         total = total + pr2[i].astype(F32)
+    recv(qp, at["qp"])
+    total = total + qp[...].astype(F32)
     proj_out[...] = total
     put(3)
 
@@ -661,16 +737,21 @@
     line, plane = pl.ds(0, s.nz - 1), pl.ds(0, s.nj - 1)
     sent(s1.at[:, line], "s1")
     sent(s2.at[:, plane], "s2")
-    for group in ("yu", "yd", "yr"):
+    for group in ("yu", "yd"):
         sent(xa.at[0, pl.ds(0, s.via), :, half(0)], group)
-    sent(xa.at[0, pl.ds(0, 6)], "rs")
+    sent(xa.at[0, pl.ds(0, s.via - 1), :, half(0)], "yr")
+    sent(xa.at[0, pl.ds(0, 5)], "rs")
+    sent(tfr, "tf")
     sent(s3.at[:, plane], "sa")
     sent(s4.at[:, line], "sb")
     sent(tg.at[pl.ds(0, 6)], "tg")
     sent(cmr.at[pl.ds(0, s.ns - 1)], "cm")
     sent(ks.at[:, :, front], "ks")
     sent(adj.at[:, front], "adj")
-    sent(pf.at[:, plane], "pj")
+    if beside:
+        sent(pf.at[:, pl.ds(0, len(beside))], "pj")
+    sent(qr.at[line], "qz")
+    sent(qs, "qp")
     sent(ps2.at[line], "pz")
 
 
@@ -704,11 +785,13 @@
         b(2, s.nk, s.sl, s.c), f(s.sl, 2 * ffl), f(s.sl, ffl), b(s.sl, 2 * ffl), b(s.sl, ffl),
         b(2, s.sl, s.c), b(2, s.hs, s.c), b(2, s.hs, s.c), b(2, s.sl, s.c), b(2, s.sl, s.c),
         f(2, s.hs, s.c), f(2, s.hs, s.c), f(2, s.sl, s.c), b(2, s.sl, s.c), b(2, s.sl, s.c),
-        b(4, s.nj, s.bl, s.w), b(4, s.nj, s.bl, s.w), b(4, s.nz, s.bl, s.w), b(4, s.nz, s.bl, s.w),
+        b(6, s.nj, s.bl, s.w), b(6, s.nj, s.bl, s.w), b(6, s.nz, s.bl, s.w), b(6, s.nz, s.bl, s.w),
+        b(2, tok, s.w), b(2, tok, s.w),
         b(s.nk, tok, s.c),
         b(4, ch, ch), f(tok, ch), f(tok, ch), b(tok, ch), f(2, nst, tok, ch), f(2, 4, tok + 8, ch),
         f(2, ch), f(2, tok + 8, ch), f(2, 2, ch), f(ns, 2, ch),
         f(2, tok + 8, ch), b(s.nz, s.nj, s.r, ch), b(s.nj, s.nz, s.r, ch), b(s.nz, s.r, ch), b(s.nz, s.r, ch),
+        b(s.nz, s.r, ch), b(s.r, ch), b(s.r, ch),
         pltpu.SemaphoreType.DMA((groups,)), pltpu.SemaphoreType.DMA((count,)),
         pltpu.SemaphoreType.DMA((16,)),
     ]

time: 112 us -> 106 us (0.946)
  Pallas kernels: 111 us -> 105 us
    pallas_call x1, Pallas kernels: 109 us -> 103 us  [on_device(): pl.pallas_call(functools.partial(kernel, s), out_shape=tuple((pltpu.VMEM(...]
where the time goes in v3:
time: 106 us; the launch traced here: 105 us
  Pallas kernels  105 us (99%)
    pallas_call x1, Pallas kernels, on_device(): pl.pallas_call(functools.partial(kernel, s), out_shape=tuple((pltpu.VMEM(...  103 us

profile of v3, /device:TPU:1, one launch (start us, length us, event | category | flops | bytes accessed | tf_op | source)
XLA Modules:
  0.0 105.5 jit_solution(14174281754885525748)
XLA Ops:
  0.6 102.9 %step.1 = (bf16[2048,256]{1,0:T(8,128)(2,1)S(1)}, bf16[2048,256]{1,0:T(8,128)(2,1)S(1)}, bf16[256,2048]{1,0:T(8,128)(2,1)S(1)}, f32[32,128]{1,0:T(8,128)S(1)}, b...) custom-call(bf16[192,2048]{1,0:T(8,128)(2,1)} %refs_0_.1, bf16[192,2048]{1,0:T(8,128)(2,1)} %refs_1_.1, ...), custom_call_target="tpu_custom_call" | custom-call | tf_op jit(solution)/shard_map/step/pallas_call | solution.py:801
  103.6 1.7 %write_out.1 = (bf16[2048,256]{1,0:T(8,128)(2,1)}, bf16[2048,256]{1,0:T(8,128)(2,1)}, bf16[256,2048]{1,0:T(8,128)(2,1)}, f32[32,128]{1,0:T(8,128)}, bf16[192,128]{1,0:T(8,128)(2,1)}, /*index=5*/bf16[192,128]{1,0:T(8,128)(2,1)}) custom-call(bf16[2048,256]{1,0:T(8,128)(2,1)S(1)} %get-tuple-element.18.refs_0_, bf16[2048,256]{1,0:T(8,128)(2,1)S(1)} %get-tuple-element.19.refs_1_, ...), custom_call_target="tpu_custom_call" | custom-call | tf_op jit(solution)/shard_map/write_out/pallas_call | solution.py:811

commit v4 on v3

--- a/solution.py
+++ b/solution.py
@@ -420,14 +420,14 @@
     relay(6)
     for place in (y, up, down):
         take_half(place, 0)
-    spread(11)
-    take_half(opp, 0)
     arrive(2)
     arrive(3)
     take(1, [opp])
     arrive(4)
     arrive(5)
     take(2, [opp])
+    spread(11)
+    take_half(opp, 0)
 
     gate_pre, up_pre = gu[:, :s.ffl], gu[:, s.ffl:]
     act_grad = ag[...]
@@ -446,8 +446,9 @@
     def partial(owner, c):
         return dot(delta[...], weights_of(owner * 2 + c), 1, 1)
 
-    def far_partial(c):
-        p2[c] = partial(opp, c).astype(BF16)
+    def far_partial(h):
+        first_row = pl.multiple_of(opp * 2 * s.c + h * s.w, s.w)
+        p2[0, :, half(h)] = dot(delta[...], wgu[pl.ds(first_row, s.w), :], 1, 1).astype(BF16)
 
     def near_partials(c):
         value = partial(up, c)
@@ -564,24 +565,24 @@
 
     far_partial(0)
     send_far(0)
+    far_partial(1)
+    send_far(1)
+    far_direct(1)
     near_partials(0)
     send_near(0)
-    send_far(1)
-    far_direct(1)
+    send_near(1)
+    near_full(1)
     own_partial(0)
-    near_full(1)
     pass_on(0)
-    send_near(1)
     own_partial(1)
-    weight_grads(0, s.nk // 4)
+    turn_back(4)
+    turn_back(5)
     pass_on(1)
     send_full(2)
     send_full(3)
-    turn_back(4)
-    turn_back(5)
-    weight_grads(s.nk // 4, s.nk // 2)
+    weight_grads(0, s.nk // 4)
     give(0)
-    weight_grads(s.nk // 2, s.nk)
+    weight_grads(s.nk // 4, s.nk)
     put(0)
     put(1)
     give(1)
@@ -594,10 +595,10 @@
     give(3)
     turn_back(2)
     combine(0)
+    turn_back(3)
+    combine(1)
     down_grads(s.nk // 2, s.nk)
     put(2)
-    turn_back(3)
-    combine(1)
     combine(2)
     combine(3)
     inv_col = inv_s[:, 0:1]
@@ -614,8 +615,8 @@
     turns = orders(s.nz) + [0]
     over = (j + s.across) % s.nj
     beside = [e for e in orders(s.nj) if e != s.across]
-    step = max(1, s.nz // 2)
-    for lot in (turns[:step], turns[step:]):
+    step = max(1, s.nz // 4)
+    for lot in [turns[i:i + step] for i in range(0, s.nz, step)]:
         for d in lot:
             zd = (z + d) % s.nz
             for i in range(per):

time: 106 us -> 105 us (level)
  no operation moved by 1% of the time
where the time goes in v4:
time: 105 us
  Pallas kernels  104 us (99%)
    pallas_call x1, Pallas kernels, on_device(): pl.pallas_call(functools.partial(kernel, s), out_shape=tuple((pltpu.VMEM(...  102 us

profile of v4, /device:TPU:1, one launch (start us, length us, event | category | flops | bytes accessed | tf_op | source)
XLA Modules:
  0.0 104.7 jit_solution(8399872563771002074)
XLA Ops:
  0.6 102.2 %step.1 = (bf16[2048,256]{1,0:T(8,128)(2,1)S(1)}, bf16[2048,256]{1,0:T(8,128)(2,1)S(1)}, bf16[256,2048]{1,0:T(8,128)(2,1)S(1)}, f32[32,128]{1,0:T(8,128)S(1)}, b...) custom-call(bf16[192,2048]{1,0:T(8,128)(2,1)} %refs_0_.1, bf16[192,2048]{1,0:T(8,128)(2,1)} %refs_1_.1, ...), custom_call_target="tpu_custom_call" | custom-call | tf_op jit(solution)/shard_map/step/pallas_call | solution.py:802
  102.8 1.7 %write_out.1 = (bf16[2048,256]{1,0:T(8,128)(2,1)}, bf16[2048,256]{1,0:T(8,128)(2,1)}, bf16[256,2048]{1,0:T(8,128)(2,1)}, f32[32,128]{1,0:T(8,128)}, bf16[192,128]{1,0:T(8,128)(2,1)}, /*index=5*/bf16[192,128]{1,0:T(8,128)(2,1)}) custom-call(bf16[2048,256]{1,0:T(8,128)(2,1)S(1)} %get-tuple-element.18.refs_0_, bf16[2048,256]{1,0:T(8,128)(2,1)S(1)} %get-tuple-element.19.refs_1_, ...), custom_call_target="tpu_custom_call" | custom-call | tf_op jit(solution)/shard_map/write_out/pallas_call | solution.py:812

commit v5 on v4

--- a/solution.py
+++ b/solution.py
@@ -79,7 +79,7 @@
 def layout(s):
     b, g = Book(), Book()
     arrivals = dict(
-        s1=b.take(s.nq), s2=b.take(s.nq), s0=b.take(s.early * (s.nj // 2)), y=b.take(3 * s.via), rs=b.take(16), sa=b.take(6),
+        s1=b.take(s.nq), s2=b.take(s.nq - s.early), s0=b.take(s.early * (s.nj // 2)), y=b.take(2 * s.via), rs=b.take(12), sa=b.take(6),
         sb=b.take(6), tf=b.take(1), tg=b.take(4), cm=b.take(1), ks=b.take(1), adj=b.take(1), pj=b.take(s.nz),
         pz=b.take(1), qz=b.take(1), qp=b.take(1),
     )
@@ -296,7 +296,7 @@
         s2[q] = blocks(dot(perm[...], flat(r1[q])))
         for d in [1] + [i for i in orders(s.nj) if i != 1]:
             jd = j ^ d
-            number = at["s0"] + q * (s.nj // 2) + j // 2 if q < s.early else at["s2"] + q
+            number = at["s0"] + q * (s.nj // 2) + j // 2 if q < s.early else at["s2"] + q - s.early
             send(s2.at[q, jd], r2.at[q, j], "s2", number, in_plane(jd))
         r2[q, j] = s2[q, j]
 
@@ -311,8 +311,8 @@
             xa[pair % 2, y * 2 + pair // 2, part, half(h)] = (
                 two[...].astype(F32).reshape(rows, s.w).astype(BF16))
             ref = tile_of(q, y).at[part]
-            send(ref, ref, "yu", at["y"] + 3 * q, on_tp(up))
-            send(ref, ref, "yd", at["y"] + 3 * q + 1, on_tp(down))
+            send(ref, ref, "yu", at["y"] + 2 * q, on_tp(up))
+            send(ref, ref, "yd", at["y"] + 2 * q, on_tp(down))
 
     top, low = pl.ds(0, s.hs), pl.ds(s.hs, s.hs)
 
@@ -324,7 +324,7 @@
         return ref.at[part]
 
     def spread(q):
-        recv(r2.at[q, pl.ds(0, s.nj - 1)], at["s2"] + q)
+        recv(r2.at[q, pl.ds(0, s.nj - 1)], at["s2"] + q - s.early)
         if q >= s.via:
             owner, h = straight(q - s.via)
             xa[1, owner * 2 + 1, :, half(h)] = flat(r2[q])
@@ -332,23 +332,22 @@
         pair, h = q // 2, q % 2
         xa[pair % 2, y * 2 + pair // 2, :, half(h)] = flat(r2[q])
         ref = tile_of(q, y)
-        n = at["y"] + 3 * q
+        n = at["y"] + 2 * q
         send(ref, ref, "yu", n, on_tp(up))
-        send(ref, ref, "yd", n + 1, on_tp(down))
+        send(ref, ref, "yd", n, on_tp(down))
 
     def relay(q):
-        n = at["y"] + 3 * q
-        ref = tile_of(q, down)
-        recv(ref, n)
+        n = at["y"] + 2 * q
+        pair, h = q // 2, q % 2
+        recv(xa.at[pair % 2, pl.ds(0, 2), :, half(h)], n)
         if q < s.via - 1:
-            send(ref.at[top], ref.at[top], "yr", n + 2, on_tp(up))
-        ref = tile_of(q, up)
-        recv(ref, n + 1)
-        if q < s.via - 1:
-            send(ref.at[low], ref.at[low], "yr", n + 2, on_tp(down))
+            ref = tile_of(q, down).at[top]
+            send(ref, ref, "yr", n + 1, on_tp(up))
+            ref = tile_of(q, up).at[low]
+            send(ref, ref, "yr", n + 1, on_tp(down))
 
     def arrive(q):
-        recv(tile_of(q, opp), at["y"] + 3 * q + 2)
+        recv(tile_of(q, opp), at["y"] + 2 * q + 1)
 
     def weights_of(k):
         return wgu[pl.ds(pl.multiple_of(k * s.c, s.c), s.c), :]
@@ -367,6 +366,18 @@
                 total[...] = value
             else:
                 total[...] += value
+
+    def slopes():
+        gate_pre, up_pre = gu[:, :s.ffl], gu[:, s.ffl:]
+        gate_clamped = jnp.minimum(gate_pre, CLAMP_LIMIT)
+        up_clamped = jnp.clip(up_pre, -CLAMP_LIMIT, CLAMP_LIMIT)
+        gate_sigmoid = jax.nn.sigmoid(SHARPNESS * gate_clamped)
+        swish_value = gate_clamped * gate_sigmoid
+        act[...] = ((up_clamped + 1.0) * swish_value).astype(BF16)
+        gate_slope = (up_clamped + 1.0) * (
+            gate_sigmoid + SHARPNESS * swish_value * (1.0 - gate_sigmoid))
+        gu[:, :s.ffl] = jnp.where(gate_pre < CLAMP_LIMIT, gate_slope, 0.0)
+        gu[:, s.ffl:] = jnp.where(jnp.abs(up_pre) < CLAMP_LIMIT, swish_value, 0.0)
 
     def take_half(place, h):
         k = place * 2 + 1
@@ -426,22 +437,13 @@
     arrive(4)
     arrive(5)
     take(2, [opp])
+    slopes()
     spread(11)
     take_half(opp, 0)
 
-    gate_pre, up_pre = gu[:, :s.ffl], gu[:, s.ffl:]
     act_grad = ag[...]
-    gate_clamped = jnp.minimum(gate_pre, CLAMP_LIMIT)
-    up_clamped = jnp.clip(up_pre, -CLAMP_LIMIT, CLAMP_LIMIT)
-    gate_sigmoid = jax.nn.sigmoid(SHARPNESS * gate_clamped)
-    swish_value = gate_clamped * gate_sigmoid
-    act[...] = ((up_clamped + 1.0) * swish_value).astype(BF16)
-    delta[:, :s.ffl] = jnp.where(
-        gate_pre < CLAMP_LIMIT,
-        act_grad * (up_clamped + 1.0)
-        * (gate_sigmoid + SHARPNESS * swish_value * (1.0 - gate_sigmoid)), 0.0).astype(BF16)
-    delta[:, s.ffl:] = jnp.where(
-        jnp.abs(up_pre) < CLAMP_LIMIT, act_grad * swish_value, 0.0).astype(BF16)
+    delta[:, :s.ffl] = (act_grad * gu[:, :s.ffl]).astype(BF16)
+    delta[:, s.ffl:] = (act_grad * gu[:, s.ffl:]).astype(BF16)
 
     def partial(owner, c):
         return dot(delta[...], weights_of(owner * 2 + c), 1, 1)
@@ -458,13 +460,16 @@
         sm1[c, :s.hs, :] = value[:s.hs].astype(BF16)
         fm[c] = value[s.hs:]
 
+    def rs_of(i):
+        return at["rs"] + (4 * i if i < 2 else 2 * i + 2)
+
     def near_full(c):
         sp1[c] = partial(up, c).astype(BF16)
         sm1[c] = partial(down, c).astype(BF16)
 
     def send_full(i):
         c, h = i // 2, half(i % 2)
-        n = at["rs"] + 4 * i
+        n = rs_of(i)
         send(sp1.at[c, :, h], rl.at[c, :, h], "rs", n + 2, on_tp(up))
         send(sm1.at[c, :, h], rr.at[c, :, h], "rs", n + 3, on_tp(down))
 
@@ -475,19 +480,19 @@
 
     def send_far(i):
         c, h = i // 2, half(i % 2)
-        n = at["rs"] + 4 * i
+        n = rs_of(i)
         send(p2.at[c, top, h], rt2.at[c, :, h], "rs", n, on_tp(up))
         send(p2.at[c, low, h], rb2.at[c, :, h], "rs", n + 1, on_tp(down))
 
     def send_near(i):
         c, h = i // 2, half(i % 2)
-        n = at["rs"] + 4 * i
+        n = rs_of(i)
         send(sp1.at[c, low, h], rl.at[c, low, h], "rs", n + 2, on_tp(up))
         send(sm1.at[c, top, h], rr.at[c, top, h], "rs", n + 3, on_tp(down))
 
     def pass_on(i):
         c, h = i // 2, half(i % 2)
-        n = at["rs"] + 4 * i
+        n = rs_of(i)
         recv(rt2.at[c, :, h], n)
         sp1[c, :s.hs, h] = (ft[c, :, h] + rt2[c, :, h].astype(F32)).astype(BF16)
         send(sp1.at[c, top, h], rl.at[c, top, h], "rs", n + 2, on_tp(up))
@@ -521,7 +526,7 @@
 
     def give(i):
         c, h = i // 2, half(i % 2)
-        n = at["rs"] + 4 * i
+        n = rs_of(i)
         recv(rl.at[c, :, h], n + 2)
         recv(rr.at[c, :, h], n + 3)
         into_plane(i, fo[c, :, h] + rl[c, :, h].astype(F32) + rr[c, :, h].astype(F32))
@@ -612,6 +617,7 @@
     inner_mean = jnp.sum(prods, axis=1, keepdims=True) * (1.0 / s.d)
     branch_grad = jnp.zeros((s.tok, s.ch), F32)
     per = s.nk // s.nz
+    kept = []
     turns = orders(s.nz) + [0]
     over = (j + s.across) % s.nj
     beside = [e for e in orders(s.nj) if e != s.across]
@@ -625,7 +631,7 @@
                 part = mid[:, cols].astype(F32) * inv_col
                 value = (og[:, cols].astype(F32)
                          + inv_col * (tg[k].astype(F32) - part * inner_mean)).astype(BF16)
-                branch_grad = branch_grad + dot(value, outp[:, cols], 1, 1)
+                kept.append((value, cols))
                 value = dot(value, mixed[...], 0, 0).astype(BF16)
                 if per == 1:
                     pf[zd] = value.reshape(s.nj, s.r, s.ch)
@@ -641,6 +647,8 @@
                 jd = (j + e) % s.nj
                 send(pf.at[zd, jd], pr.at[j, zd], "pj", at["pj"] + zd, in_plane(jd))
             pr[j, zd] = pf[zd, j]
+    for value, cols in kept:
+        branch_grad = branch_grad + dot(value, outp[:, cols], 1, 1)
     bgg_out[...] = (branch_grad * sslope[...]).astype(BF16)
     put(5)
     state_grad = branch_grad * gel[...]
@@ -814,7 +822,7 @@
         out_shape=tuple(jax.ShapeDtypeStruct(*x) for x in shapes),
         in_specs=[hbm] * 6,
         out_specs=(hbm,) * 6,
-        scratch_shapes=[pltpu.SemaphoreType.DMA((6,))],
+        scratch_shapes=[pltpu.SemaphoreType.DMA((15,))],
         compiler_params=pltpu.CompilerParams(vmem_limit_bytes=1024 * 1024),
         name="write_out",
     )(*(pltpu.with_memory_space_constraint(x, pltpu.VMEM) for x in outs))
@@ -823,7 +831,14 @@
 
 
 def write_out(*refs):
-    copies = [pltpu.make_async_copy(refs[i], refs[6 + i], refs[12].at[i]) for i in range(6)]
+    copies = []
+    for i in range(6):
+        parts = 4 if i < 3 else 1
+        rows = refs[i].shape[0] // parts
+        for n in range(parts):
+            part = pl.ds(n * rows, rows)
+            copies.append(pltpu.make_async_copy(
+                refs[i].at[part], refs[6 + i].at[part], refs[12].at[len(copies)]))
     for cp in copies:
         cp.start()
     for cp in copies:

time: 105 us -> 104 us (level)
  no operation moved by 1% of the time
where the time goes in v5:
time: 104 us
  Pallas kernels  104 us (100%)
    pallas_call x1, Pallas kernels, on_device(): pl.pallas_call(functools.partial(kernel, s), out_shape=tuple((pltpu.VMEM(...  102 us

profile of v5, /device:TPU:1, one launch (start us, length us, event | category | flops | bytes accessed | tf_op | source)
XLA Modules:
  0.0 104.4 jit_solution(8158312561084684167)
XLA Ops:
  0.6 101.7 %step.1 = (bf16[2048,256]{1,0:T(8,128)(2,1)S(1)}, bf16[2048,256]{1,0:T(8,128)(2,1)S(1)}, bf16[256,2048]{1,0:T(8,128)(2,1)S(1)}, f32[32,128]{1,0:T(8,128)S(1)}, b...) custom-call(bf16[192,2048]{1,0:T(8,128)(2,1)} %refs_0_.1, bf16[192,2048]{1,0:T(8,128)(2,1)} %refs_1_.1, ...), custom_call_target="tpu_custom_call" | custom-call | tf_op jit(solution)/shard_map/step/pallas_call | solution.py:810
  102.4 1.8 %write_out.1 = (bf16[2048,256]{1,0:T(8,128)(2,1)}, bf16[2048,256]{1,0:T(8,128)(2,1)}, bf16[256,2048]{1,0:T(8,128)(2,1)}, f32[32,128]{1,0:T(8,128)}, bf16[192,128]{1,0:T(8,128)(2,1)}, /*index=5*/bf16[192,128]{1,0:T(8,128)(2,1)}) custom-call(bf16[2048,256]{1,0:T(8,128)(2,1)S(1)} %get-tuple-element.18.refs_0_, bf16[2048,256]{1,0:T(8,128)(2,1)S(1)} %get-tuple-element.19.refs_1_, ...), custom_call_target="tpu_custom_call" | custom-call | tf_op jit(solution)/shard_map/write_out/pallas_call | solution.py:820
